TPU v7x, 32 devices: a whole 2x2x4 slice. The times are simulated.
32 devices in a mesh: sp: 8 (over z, core), tp: 4 (over y, x).
Axes of the slice: x: 2, y: 2, z: 4, core: 2. Of those that a mesh axis runs over, the one named last changes fastest.
Arguments:
- resid: bfloat16 [2048, 2048], P('sp'), may hold values from -18 to 18
- narrow_head_input: bfloat16 [2048, 1024], P('sp', 'tp'), may hold values from -6 to 6
- wide_head_input: bfloat16 [2048, 2048], P('sp', 'tp'), may hold values from -6 to 6
- key_group_input: bfloat16 [2048, 512], P('sp'), may hold values from -6 to 6
- query_group_input: bfloat16 [2048, 512], P('sp'), may hold values from -6 to 6
- narrow_output_gate: bfloat16 [2048, 1024], P('sp', 'tp'), may hold values from -6 to 6
- wide_output_gate: bfloat16 [2048, 2048], P('sp', 'tp'), may hold values from -6 to 6
- step_input_rows: bfloat16 [2048, 2, 16], P('sp', None, 'tp'), may hold values from -4 to 4
- head_decay_logarithm: float32 [2, 16], P(None, 'tp'), may hold values from -14 to -2
- position_log_decay: float32 [2048, 2, 16], P('sp', None, 'tp'), may hold values from -1.4 to 0
- direct_input_weight: float32 [2, 16], P(None, 'tp'), may hold values from 0.5 to 2
- narrow_conv_taps: float32 [4, 1024], P(None, 'tp'), may hold values from -3 to 3
- wide_conv_taps: float32 [4, 2048], P(None, 'tp'), may hold values from -3 to 3
- key_conv_taps: float32 [4, 512], replicated, may hold values from -3 to 3
- query_conv_taps: float32 [4, 512], replicated, may hold values from -3 to 3
- narrow_norm_gain: float32 [1024], P('tp'), may hold values from 0.1 to 1.9
- wide_norm_gain: float32 [2048], P('tp'), may hold values from 0.1 to 1.9
- narrow_output_rows: bfloat16 [1024, 2048], P('tp'), may hold values from -0.109375 to 0.109375
- wide_output_rows: bfloat16 [2048, 2048], P('tp'), may hold values from -0.109375 to 0.109375
- feedforward_norm_gain: float32 [2048], replicated, may hold values from 0.1 to 1.9
- routes: int32 [2048, 3], P('sp'), may hold values from 0 to 7, all different within a row; in each aligned block of 256 rows (0 to 255, 256 to 511, ...) at most 128 rows name the same one
- routing_weight_values: float32 [2048, 3], P('sp'), may hold values from 0.1 to 1
- expert_gate_matrix: bfloat16 [8, 2048, 2048], P('sp', None, 'tp'), may hold values from -1 to 1
- expert_up_matrix: bfloat16 [8, 2048, 2048], P('sp', None, 'tp'), may hold values from -1 to 1
- expert_down_matrix: bfloat16 [8, 2048, 2048], P('sp', 'tp'), may hold values from -0.015625 to 0.015625
Outputs:
- layer_out: bfloat16 [2048, 2048], P('sp', 'tp')
Inputs may be any that keep to these rules, and one draw needn't show every extreme that they name: `routes`: each token names 3 different experts. Among the tokens of one index of sp (aligned blocks of 256 rows) no expert is named by more than 128 of them, and in some blocks one is named by exactly 128.
All inputs are finite; a program needn't handle non-finite values.
Results may differ from a plain program's by a relative error of at most 0.015.
Values may be sent and summed in bfloat16 or wider, within the bound.
No kernel may reach another device: no remote copies, remote signals or barrier semaphores. Data moves between devices by JAX's collectives and lax.ppermute only.
A program may use at most 64 MiB of HBM per device.

v0:
```python
import functools

import jax
import jax.numpy as jnp
from jax import lax
from jax.sharding import PartitionSpec as P

HEADS = 16
NARROW_HEAD_DIM = 64
WIDE_HEAD_DIM = 128
GROUPS = 4
BLOCK = 128


NORM_EPS = 1e-06
CLAMP_LIMIT = 7.0
SIGMOID_SCALE = 1.702
FULL_PRECISION = lax.Precision.HIGHEST


def passed_along(block, axis, distance):
    devices = range(lax.axis_size(axis))
    route = [(i - distance, i) for i in devices if i - distance in devices]
    return lax.ppermute(block, axis, route)


def entering_2(x, axis, join, neutral):
    place = lax.axis_index(axis)
    gathered = jax.tree.map(
        lambda a, kind: lax.all_gather(a.astype(kind), axis),
        x,
        jax.tree.map(lambda a: jnp.bfloat16 if a.dtype == jnp.float32 else a.dtype, x),
    )
    state = jax.tree.map(lambda a, e: jnp.zeros_like(a) + jnp.asarray(e, a.dtype), x, neutral)

    def one(lap, state):
        return join(
            state,
            jax.tree.map(
                lambda a, own: lax.dynamic_index_in_dim(a, lap, 0, False).astype(own.dtype),
                gathered,
                x,
            ),
        )

    return lax.fori_loop(0, place, one, state)


def conv_with_rim(values, rim_rows, weight):
    length = values.shape[0]
    padded = jnp.concatenate([rim_rows, values], axis=0).astype(jnp.float32)
    accumulated = jnp.zeros((length, values.shape[1]), jnp.float32)
    for tap_index in range(weight.shape[0]):
        accumulated = accumulated + weight[tap_index] * padded[tap_index : tap_index + length]
    return jax.nn.silu(accumulated)


def pick_groups(channel_table, first_head, head_count):
    length = channel_table.shape[0]
    grouped = channel_table.reshape(length, GROUPS, -1)
    owners = (first_head + jnp.arange(head_count, dtype=jnp.int32)) // (HEADS // GROUPS)
    chooser = (owners[:, None] == jnp.arange(GROUPS, dtype=jnp.int32)[None, :]).astype(jnp.float32)
    return jnp.einsum("sgn,hg->shn", grouped, chooser, precision=FULL_PRECISION)


def local_head(values, step_logarithm, key_head_rows, query_head_rows, block_len):
    block_count = values.shape[0] // block_len
    values = values.reshape(block_count, block_len, -1)
    step_logarithm = step_logarithm.reshape(block_count, block_len)
    key_head_rows = key_head_rows.reshape(block_count, block_len, -1)
    query_head_rows = query_head_rows.reshape(block_count, block_len, -1)
    cum_decay = jnp.cumsum(step_logarithm, axis=1)
    causal_mask = jnp.arange(block_len)[:, None] >= jnp.arange(block_len)[None, :]
    decay_gaps = jnp.where(causal_mask[None], cum_decay[:, :, None] - cum_decay[:, None, :], -1e30)
    scores = jnp.einsum(
        "bln,bsn->bls", query_head_rows, key_head_rows, precision=FULL_PRECISION
    ) * jnp.exp(decay_gaps)
    inside = jnp.einsum("bls,bsp->blp", scores, values, precision=FULL_PRECISION)
    tail_decay = jnp.exp(cum_decay[:, -1:] - cum_decay)
    states = jnp.einsum(
        "bln,blp->bnp", key_head_rows * tail_decay[..., None], values, precision=FULL_PRECISION
    )
    totals = cum_decay[:, -1]

    def walk(running, member):
        return (jnp.exp(member[1]) * running + member[0], running)

    closing, entering = lax.scan(walk, jnp.zeros(states.shape[1:], jnp.float32), (states, totals))
    before = jnp.cumsum(totals) - totals
    return (inside, entering, closing, jnp.sum(totals), before, cum_decay, query_head_rows)


def finish_head(inside, entering, before, cum_decay, query_blocks, carried):
    starting = entering + jnp.exp(before)[:, None, None] * carried[None]
    readout = jnp.einsum(
        "bln,bnp->blp",
        query_blocks * jnp.exp(cum_decay)[..., None],
        starting,
        precision=FULL_PRECISION,
    )
    return (inside + readout).reshape(-1, inside.shape[-1])


def group_out(scanned, mixed_input_rows, direct_input_term, gate_input_rows, norm_gain_vector):
    length, head_count, head_dimension = mixed_input_rows.shape
    gated = jax.nn.silu(gate_input_rows.astype(jnp.float32)).reshape(
        length, head_count, head_dimension
    )
    result = (scanned + direct_input_term[None, :, None] * mixed_input_rows) * gated
    result = result * lax.rsqrt(jnp.mean(result * result, axis=-1, keepdims=True) + NORM_EPS)
    return (result.reshape(length, head_count * head_dimension) * norm_gain_vector).astype(
        jnp.bfloat16
    )


def head_pieces_list(
    mixed_input_rows,
    step_length_values,
    decay_vector,
    position_decay_rows,
    key_head_rows,
    query_head_rows,
):
    step_logarithm = -jnp.exp(decay_vector)[None, :] * step_length_values + position_decay_rows
    values = mixed_input_rows * step_length_values[..., None]
    walker = functools.partial(local_head, block_len=BLOCK)
    return jax.vmap(walker, in_axes=(1, 1, 1, 1))(
        values, step_logarithm, key_head_rows, query_head_rows
    )


def finish_group(parts, carried_states):
    return jax.vmap(finish_head, in_axes=(0, 0, 0, 0, 0, 0), out_axes=1)(
        parts[0], parts[1], parts[4], parts[5], parts[6], carried_states
    )


def chain_combine(earlier, later):
    return (
        earlier[0] + later[0],
        earlier[1] + later[1],
        jnp.exp(later[0])[:, None, None] * earlier[2] + later[2],
        jnp.exp(later[1])[:, None, None] * earlier[3] + later[3],
    )


def local(
    resid,
    narrow_head_input,
    wide_head_input,
    key_group_input,
    query_group_input,
    narrow_output_gate,
    wide_output_gate,
    step_input_rows,
    head_decay_logarithm,
    position_log_decay,
    direct_input_weight,
    narrow_conv_taps,
    wide_conv_taps,
    key_conv_taps,
    query_conv_taps,
    narrow_norm_gain,
    wide_norm_gain,
    narrow_output_rows,
    wide_output_rows,
    feedforward_norm_gain,
    routes,
    routing_weight_values,
    expert_gate_matrix,
    expert_up_matrix,
    expert_down_matrix,
):
    length = resid.shape[0]
    head_count = narrow_head_input.shape[1] // NARROW_HEAD_DIM
    rim_len = narrow_conv_taps.shape[0] - 1
    rim_rows = passed_along(
        (
            narrow_head_input[length - rim_len :],
            wide_head_input[length - rim_len :],
            key_group_input[length - rim_len :],
            query_group_input[length - rim_len :],
        ),
        "sp",
        1,
    )
    narrow_head_mix = conv_with_rim(narrow_head_input, rim_rows[0], narrow_conv_taps).reshape(
        length, head_count, NARROW_HEAD_DIM
    )
    wide_head_mix = conv_with_rim(wide_head_input, rim_rows[1], wide_conv_taps).reshape(
        length, head_count, WIDE_HEAD_DIM
    )
    first_head = lax.axis_index("tp") * head_count
    key_head_rows = pick_groups(
        conv_with_rim(key_group_input, rim_rows[2], key_conv_taps), first_head, head_count
    )
    query_head_rows = pick_groups(
        conv_with_rim(query_group_input, rim_rows[3], query_conv_taps), first_head, head_count
    )
    step_length_values = jax.nn.softplus(step_input_rows.astype(jnp.float32))
    narrow_parts = head_pieces_list(
        narrow_head_mix,
        step_length_values[:, 0],
        head_decay_logarithm[0],
        position_log_decay[:, 0],
        key_head_rows,
        query_head_rows,
    )
    wide_parts = head_pieces_list(
        wide_head_mix,
        step_length_values[:, 1],
        head_decay_logarithm[1],
        position_log_decay[:, 1],
        key_head_rows,
        query_head_rows,
    )
    summary = (narrow_parts[3], wide_parts[3], narrow_parts[2], wide_parts[2])
    carried = entering_2(
        summary,
        "sp",
        chain_combine,
        (
            jnp.zeros_like(summary[0]),
            jnp.zeros_like(summary[1]),
            jnp.zeros_like(summary[2]),
            jnp.zeros_like(summary[3]),
        ),
    )
    narrow_carry, wide_carry = (carried[2], carried[3])
    narrow_head_output = group_out(
        finish_group(narrow_parts, narrow_carry),
        narrow_head_mix,
        direct_input_weight[0],
        narrow_output_gate,
        narrow_norm_gain,
    )
    wide_head_output = group_out(
        finish_group(wide_parts, wide_carry),
        wide_head_mix,
        direct_input_weight[1],
        wide_output_gate,
        wide_norm_gain,
    )
    partial_mix = jnp.dot(
        narrow_head_output, narrow_output_rows, preferred_element_type=jnp.float32
    )
    partial_mix = partial_mix + jnp.dot(
        wide_head_output, wide_output_rows, preferred_element_type=jnp.float32
    )
    mixed = lax.psum(partial_mix.astype(jnp.bfloat16), "tp").astype(jnp.float32)
    hidden_state = resid.astype(jnp.float32) + mixed
    normed = (
        hidden_state
        * lax.rsqrt(jnp.mean(hidden_state * hidden_state, axis=-1, keepdims=True) + NORM_EPS)
        * feedforward_norm_gain
    ).astype(jnp.bfloat16)
    experts = lax.axis_size("sp")
    picks = routes.shape[1]
    capacity = 4 * length * picks // (3 * experts)
    column_width = normed.shape[1] // lax.axis_size("tp")
    tp_index = lax.axis_index("tp")
    flat_routes = routes.reshape(-1)
    member_hits = (flat_routes[:, None] == jnp.arange(experts, dtype=jnp.int32)[None, :]).astype(
        jnp.int32
    )
    ranks = jnp.sum((jnp.cumsum(member_hits, axis=0) - member_hits) * member_hits, axis=1)
    slot_ids = flat_routes * capacity + ranks
    source_rows = (
        jnp.zeros((experts * capacity,), jnp.int32)
        .at[slot_ids]
        .set(jnp.arange(length * picks, dtype=jnp.int32) // picks)
    )
    occupied = jnp.zeros((experts * capacity,), jnp.int32).at[slot_ids].set(1)
    gate_weight = expert_gate_matrix[0]
    up_weight = expert_up_matrix[0]
    down_weight = expert_down_matrix[0]
    own_columns = lax.dynamic_slice_in_dim(normed, tp_index * column_width, column_width, 1)
    outgoing = jnp.where(
        occupied[:, None] > 0, own_columns[source_rows], jnp.zeros((), jnp.bfloat16)
    )
    arrived = lax.all_to_all(
        outgoing.reshape(experts, capacity, column_width),
        "sp",
        split_axis=0,
        concat_axis=0,
        tiled=True,
    )
    slot_parts = arrived.reshape(experts * capacity, column_width)
    piece = lax.all_gather(slot_parts, "tp", axis=1, tiled=True)
    gate_pre = jnp.dot(piece, gate_weight, preferred_element_type=jnp.float32)
    up_pre = jnp.dot(piece, up_weight, preferred_element_type=jnp.float32)
    clamped = jnp.minimum(gate_pre, CLAMP_LIMIT)
    act = (
        (jnp.clip(up_pre, -CLAMP_LIMIT, CLAMP_LIMIT) + 1.0)
        * clamped
        * jax.nn.sigmoid(SIGMOID_SCALE * clamped)
    ).astype(jnp.bfloat16)
    partial_out = jnp.dot(act, down_weight, preferred_element_type=jnp.float32)
    summed = lax.psum_scatter(
        partial_out.reshape(experts, capacity, -1).astype(jnp.bfloat16),
        "tp",
        scatter_dimension=2,
        tiled=True,
    )
    returned = lax.all_to_all(summed, "sp", split_axis=0, concat_axis=0, tiled=True)
    token_rows = returned.reshape(experts * capacity, -1)[slot_ids].reshape(length, picks, -1)
    combined = jnp.sum(token_rows.astype(jnp.float32) * routing_weight_values[..., None], axis=1)
    own_state = lax.dynamic_slice_in_dim(hidden_state, tp_index * column_width, column_width, 1)
    return (own_state + combined).astype(jnp.bfloat16)


def solution(mesh):
    return jax.shard_map(
        local,
        mesh=mesh,
        in_specs=(
            P("sp", None),
            P("sp", "tp"),
            P("sp", "tp"),
            P("sp", None),
            P("sp", None),
            P("sp", "tp"),
            P("sp", "tp"),
            P("sp", None, "tp"),
            P(None, "tp"),
            P("sp", None, "tp"),
            P(None, "tp"),
            P(None, "tp"),
            P(None, "tp"),
            P(),
            P(),
            P("tp"),
            P("tp"),
            P("tp", None),
            P("tp", None),
            P(),
            P("sp", None),
            P("sp", None),
            P("sp", None, "tp"),
            P("sp", None, "tp"),
            P("sp", "tp", None),
        ),
        out_specs=P("sp", "tp"),
        check_vma=False,
    )
```

profile of v0, /device:TPU:0, one launch (start us, length us, event | category | flops | bytes accessed | tf_op | source)
XLA Modules:
  0.0 406.6 jit_solution(8500874269213244223)
XLA Ops:
  6.5 1.4 slice.156
  8.0 3.0 collective-permute-start.1
  11.8 4.6 %collective-permute-start.2 = (bf16[3,256]{0,1:T(8,128)(2,1)S(1)}, bf16[3,256]{0,1:T(8,128)(2,1)}, u32[]{:S(2)}, u32[]{:S(2)}) collective-permute-start(bf16[3,256]{0,1:T(8,128)(2,1)S(1)} %copy.90), channel_id=1, source_target_pairs={{0,4},{4,8},{8,12},{12,16},{16,20},{20,24},{24,28},{1,5},{5,9},{9,... | collective-permute-start | bytes 4616 | tf_op jit(solution)/shard_map/ppermute | solution.py:24
  16.4 1.3 slice.182
  17.7 1.9 collective-permute-start.3
  19.6 1.3 slice.147
  20.9 3.6 collective-permute-start
  24.5 1.7 copy.91
  29.1 1.2 reduce_window_sum.49
  30.3 1.2 reduce_window_sum.51
  33.9 1.5 fusion.104
  35.9 1.4 fusion.108
  37.4 1.5 fusion.103
  38.8 1.5 fusion.102
  40.9 1.3 slice_bitcast_fusion.2
  42.2 1.1 convert_multiply_fusion
  43.9 1.3 dynamic-slice
  46.2 13.6 %all-reduce.2 = (bf16[32]{0:T(256)(128)(2,1)S(1)}, bf16[32]{0:T(256)(128)(2,1)S(1)}) all-reduce(bf16[32]{0:T(256)(128)(2,1)S(1)} %dynamic-update-slice, bf16[32]{0:T(256)(128)(2,1)S(1)} %dynamic-update-slice.1), channel_id=2, replica_groups=mesh['sp'=8,'tp'=4] {'sp'}, use_global_device_ids=true, to_apply=%add | all-reduce | flops 64 | bytes 256
  62.8 1.0 copy.118
  65.5 1.0 maximum_convert_fusion.3
  66.6 1.8 divide_multiply_fusion.3
  68.4 1.0 maximum_convert_fusion.1
  69.4 1.0 divide_multiply_fusion.1
  70.4 1.0 reshape.264
  71.4 1.0 maximum_convert_fusion.2
  72.5 1.8 divide_multiply_fusion
  74.3 1.2 copy.104
  75.5 1.5 multiply_bitcast_fusion
  77.1 2.1 copy.128
  79.1 3.0 broadcast_multiply_fusion.2
  82.1 1.0 convolution_bitcast_fusion
  83.2 3.1 while.44
  87.0 1.7 convolution_bitcast_fusion.1
  88.7 3.4 while.43
  92.2 1.0 maximum_convert_fusion
  94.6 17.4 %all-gather.1 = bf16[32,128,64]{1,2,0:T(8,128)(2,1)} all-gather(bf16[4,128,64]{1,2,0:T(8,128)(2,1)S(1)} %copy.100), channel_id=3, replica_groups=mesh['sp'=8,'tp'=4] {'sp'}, dimensions={0}, use_global_device_ids=true | all-gather | bytes 589824 | tf_op jit(solution)/shard_map/all_gather | solution.py:30
  112.1 3.0 broadcast_multiply_fusion.1
  115.1 1.2 fusion.40
  117.1 1.6 fusion.43
  119.0 2.9 convolution_add_fusion.1
  121.9 2.0 copy.117
  124.0 1.5 multiply_reduce_fusion.2
  125.6 1.1 fusion.33
  126.8 1.2 fusion.18
  130.5 1.7 fusion.10
  132.5 1.7 reduce-window.6
  135.1 3.4 scatter_custom_fusion.1
  138.5 3.4 scatter_custom_fusion
  142.7 60.3 %all-reduce.5.cloned.1.call-done = bf16[256,2048]{1,0:T(8,128)(2,1)} async-done(((bf16[256,2048]{1,0:T(8,128)(2,1)}), bf16[256,2048]{1,0:T(8,128)(2,1)}) %all-reduce.5.cloned.1.call-update) | async-done | bytes 1048592 | tf_op jit(solution)/shard_map/psum | solution.py:250
  203.0 1.6 multiply_reduce_fusion.1
  204.6 1.4 copy-done.3
  206.1 4.0 gather_fusion
  210.3 31.1 %all_to_all.10 = bf16[8,128,512]{2,1,0:T(8,128)(2,1)} all-to-all(bf16[8,128,512]{2,1,0:T(8,128)(2,1)S(1)} %broadcast_select_fusion), channel_id=1, replica_groups=mesh['sp'=8,'tp'=4] {'sp'}, dimensions={0} | all-to-all | bytes 2097152 | tf_op jit(solution)/shard_map/all_to_all | solution.py:281
  241.7 50.3 %all-gather.7.cloned.1.call-done = bf16[1024,2048]{1,0:T(8,128)(2,1)} async-done(((bf16[1024,512]{1,0:T(8,128)(2,1)}), bf16[1024,2048]{1,0:T(8,128)(2,1)}) %all-gather.7.cloned.1.call-update) | async-done | bytes 4194320 | tf_op jit(solution)/shard_map/all_gather | solution.py:289
  291.9 5.3 %fusion.14 = f32[1024,512]{1,0:T(8,128)S(1)} fusion(bf16[1024,2048]{1,0:T(8,128)(2,1)} %all-gather.7.cloned.1.call-done, bf16[1,2048,512]{2,1,0:T(8,128)(2,1)} %param.54), kind=kOutput, calls=%fused_computation.32 | convolution fusion | flops 2147483648 | bytes 8388608 | tf_op jit(solution)/shard_map/dot_general | solution.py:291
  297.3 2.8 multiply_convert_fusion
  300.2 4.3 %convolution_convert_fusion = bf16[8,128,2048]{2,1,0:T(8,128)(2,1)} fusion(bf16[8,128,512]{2,1,0:T(8,128)(2,1)S(1)} %bitcast.258, bf16[1,512,2048]{2,1,0:T(8,128)(2,1)S(1)} %copy-done), kind=kOutput, calls=%fused_computation.26 | convolution fusion | flops 2149580800 | bytes 7340032 | tf_op jit(solution)/shard_map/dot_general | solution.py:298
  304.5 52.7 %reduce-scatter.2.cloned.1.call-done = bf16[8,128,512]{2,1,0:T(8,128)(2,1)} async-done(((bf16[8,128,2048]{2,1,0:T(8,128)(2,1)}), bf16[8,128,512]{2,1,0:T(8,128)(2,1)}) %reduce-scatter.2.cloned.1.call-update) | async-done | bytes 1048592 | tf_op jit(solution)/shard_map/reduce_scatter | solution.py:299
  357.3 4.6 %all-to-all-start.1 = ((bf16[8,128,512]{2,1,0:T(8,128)(2,1)}), bf16[8,128,512]{2,1,0:T(8,128)(2,1)S(1)}, u32[]{:S(2)}, u32[]{:S(2)}) async-start(bf16[8,128,512]{2,1,0:T(8,128)(2,1)} %reduce-scatter.2.cloned.1.call-done), calls=%async_computation.2 | async-start | bytes 2097152 | tf_op jit(solution)/shard_map/all_to_all | solution.py:305
  362.0 26.4 %all-to-all-done.1 = bf16[8,128,512]{2,1,0:T(8,128)(2,1)S(1)} async-done(((bf16[8,128,512]{2,1,0:T(8,128)(2,1)}), bf16[8,128,512]{2,1,0:T(8,128)(2,1)S(1)}, u32[]{:S(2)}, u32[]{:S(2)}) %all-to-all-start.1) | async-done | bytes 1048608 | tf_op jit(solution)/shard_map/all_to_all | solution.py:305
  388.4 3.3 gather_fusion.1
  391.8 3.5 reshape.282
  395.2 2.9 multiply_reduce_fusion
  398.2 1.8 add_convert_fusion
  (196 shorter events, 27.6 us)
Async XLA Ops:
  6.5 293.6 %copy-start = (bf16[1,512,2048]{2,1,0:T(8,128)(2,1)S(1)}, bf16[1,512,2048]{2,1,0:T(8,128)(2,1)}, u32[]{:S(2)}) copy-start(bf16[1,512,2048]{2,1,0:T(8,128)(2,1)} %param.55) | copy-start | bytes 6291460
  6.5 57.3 %copy-start.18 = (bf16[256,256]{1,0:T(8,128)(2,1)S(1)}, bf16[256,256]{1,0:T(8,128)(2,1)}, u32[]{:S(2)}) copy-start(bf16[256,256]{1,0:T(8,128)(2,1)} %param.36) | copy-start | bytes 393220
  6.5 58.0 %copy-start.29 = (s32[256,3]{0,1:T(4,128)S(1)}, s32[256,3]{0,1:T(4,128)}, u32[]{:S(2)}) copy-start(s32[256,3]{0,1:T(4,128)} %param.51) | copy-start | bytes 9220
  6.5 112.2 %all-gather.9.cloned.1.call-start = ((), (), s32[]{:S(2)}) async-start(), calls=%async_computation.6 | async-start | bytes 1179648 | tf_op jit(solution)/shard_map/all_gather | solution.py:30
  8.0 60.4 %collective-permute-start.1 = (bf16[3,512]{1,0:T(4,128)(2,1)}, bf16[3,512]{1,0:T(4,128)(2,1)}, u32[]{:S(2)}, u32[]{:S(2)}) collective-permute-start(bf16[3,512]{1,0:T(4,128)(2,1)} %slice.156), channel_id=1, source_target_pairs={{0,4},{4,8},{8,12},{12,16},{16,20},{20,24},{24,28},{1,5},{5,9},{9,... | collective-permute-start | bytes 9224 | tf_op jit(solution)/shard_map/ppermute | solution.py:24
  11.8 53.7 %collective-permute-start.2 = (bf16[3,256]{0,1:T(8,128)(2,1)S(1)}, bf16[3,256]{0,1:T(8,128)(2,1)}, u32[]{:S(2)}, u32[]{:S(2)}) collective-permute-start(bf16[3,256]{0,1:T(8,128)(2,1)S(1)} %copy.90), channel_id=1, source_target_pairs={{0,4},{4,8},{8,12},{12,16},{16,20},{20,24},{24,28},{1,5},{5,9},{9,... | collective-permute-start | bytes 4616 | tf_op jit(solution)/shard_map/ppermute | solution.py:24
  17.7 53.7 %collective-permute-start.3 = (bf16[3,512]{1,0:T(4,128)(2,1)}, bf16[3,512]{1,0:T(4,128)(2,1)}, u32[]{:S(2)}, u32[]{:S(2)}) collective-permute-start(bf16[3,512]{1,0:T(4,128)(2,1)} %slice.182), channel_id=1, source_target_pairs={{0,4},{4,8},{8,12},{12,16},{16,20},{20,24},{24,28},{1,5},{5,9},{9,... | collective-permute-start | bytes 9224 | tf_op jit(solution)/shard_map/ppermute | solution.py:24
  20.9 71.3 %collective-permute-start = (bf16[3,512]{1,0:T(4,128)(2,1)}, bf16[3,512]{1,0:T(4,128)(2,1)}, u32[]{:S(2)}, u32[]{:S(2)}) collective-permute-start(bf16[3,512]{1,0:T(4,128)(2,1)} %slice.147), channel_id=1, source_target_pairs={{0,4},{4,8},{8,12},{12,16},{16,20},{20,24},{24,28},{1,5},{5,9},{9,... | collective-permute-start | bytes 9224 | tf_op jit(solution)/shard_map/ppermute | solution.py:24
  30.3 35.2 %copy-start.21 = (f32[4,2,128]{2,1,0:T(2,128)}, f32[4,2,128]{2,1,0:T(2,128)S(1)}, u32[]{:S(2)}) copy-start(f32[4,2,128]{2,1,0:T(2,128)S(1)} %reduce_window_sum.49) | copy-start | bytes 12292
  31.5 34.0 %copy-start.23 = (f32[4,2,128]{2,1,0:T(2,128)}, f32[4,2,128]{2,1,0:T(2,128)S(1)}, u32[]{:S(2)}) copy-start(f32[4,2,128]{2,1,0:T(2,128)S(1)} %reduce_window_sum.51) | copy-start | bytes 12292
  31.8 33.7 %copy-start.28 = (f32[4,2,1]{0,1,2:T(2,128)}, f32[4,2,1]{0,1,2:T(2,128)S(1)}, u32[]{:S(2)}) copy-start(f32[4,2,1]{0,1,2:T(2,128)S(1)} %copy.101) | copy-start | bytes 100
  32.0 33.5 %copy-start.27 = (f32[4,2,1]{0,1,2:T(2,128)}, f32[4,2,1]{0,1,2:T(2,128)S(1)}, u32[]{:S(2)}) copy-start(f32[4,2,1]{0,1,2:T(2,128)S(1)} %copy.94) | copy-start | bytes 100
  64.7 0.8 copy-start.10
  75.5 6.6 %copy-start.4 = (f32[256,512]{0,1:T(8,128)}, f32[256,512]{0,1:T(8,128)S(1)}, u32[]{:S(2)}) copy-start(f32[256,512]{0,1:T(8,128)S(1)} %copy.104) | copy-start | bytes 1572868
  79.1 3.0 copy-start.1
  86.9 116.0 %all-reduce.5.cloned.1.call-start = ((), (), s32[]{:S(2)}) async-start(), calls=%async_computation.3 | async-start | bytes 2097152 | tf_op jit(solution)/shard_map/psum | solution.py:250
  88.7 4.6 %copy-start.35 = (f32[1,512]{1,0:T(1,128)S(1)}, f32[1,512]{1,0:T(1,128)}, u32[]{:S(2)}) copy-start(f32[1,512]{1,0:T(1,128)} %get-tuple-element.285) | copy-start | bytes 6148
  88.7 4.6 %copy-start.36 = (f32[1,512]{1,0:T(1,128)S(1)}, f32[1,512]{1,0:T(1,128)}, u32[]{:S(2)}) copy-start(f32[1,512]{1,0:T(1,128)} %get-tuple-element.286) | copy-start | bytes 6148
  88.7 4.6 %copy-start.37 = (f32[1,512]{1,0:T(1,128)S(1)}, f32[1,512]{1,0:T(1,128)}, u32[]{:S(2)}) copy-start(f32[1,512]{1,0:T(1,128)} %get-tuple-element.287) | copy-start | bytes 6148
  88.7 4.6 %copy-start.38 = (f32[1,512]{1,0:T(1,128)S(1)}, f32[1,512]{1,0:T(1,128)}, u32[]{:S(2)}) copy-start(f32[1,512]{1,0:T(1,128)} %get-tuple-element.288) | copy-start | bytes 6148
  93.3 18.7 %copy-start.19 = (f32[4,2,128]{0,2,1:T(8,128)S(1)}, f32[4,2,128]{0,2,1:T(8,128)}, u32[]{:S(2)}) copy-start(f32[4,2,128]{0,2,1:T(8,128)} %copy.93) | copy-start | bytes 12292
  93.3 18.7 %copy-start.20 = (f32[4,2,128]{0,2,1:T(8,128)S(1)}, f32[4,2,128]{0,2,1:T(8,128)}, u32[]{:S(2)}) copy-start(f32[4,2,128]{0,2,1:T(8,128)} %copy.114) | copy-start | bytes 12292
  93.3 18.7 %copy-start.46 = (s32[4]{0:T(128)S(1)}, s32[4]{0:T(128)}, u32[]{:S(2)}) copy-start(s32[4]{0:T(128)} %and_select_fusion) | copy-start | bytes 52
  112.0 3.0 copy-start.14
  112.0 5.1 %copy-start.2 = (f32[4,256,128]{2,1,0:T(8,128)S(1)}, f32[4,256,128]{2,1,0:T(8,128)}, u32[]{:S(2)}) copy-start(f32[4,256,128]{2,1,0:T(8,128)} %copy.128) | copy-start | bytes 1572868
  112.1 5.0 %copy-start.24 = (f32[4,2,128]{2,1,0:T(2,128)S(1)}, f32[4,2,128]{2,1,0:T(2,128)}, u32[]{:S(2)}) copy-start(f32[4,2,128]{2,1,0:T(2,128)} %copy-done.23) | copy-start | bytes 12292
  116.3 0.8 copy-start.6
  119.0 5.0 %copy-start.5 = (f32[256,512]{0,1:T(8,128)S(1)}, f32[256,512]{0,1:T(8,128)}, u32[]{:S(2)}) copy-start(f32[256,512]{0,1:T(8,128)} %copy-done.4) | copy-start | bytes 1572868
  121.9 3.7 copy-start.40
  123.9 1.6 copy-start.16
  123.9 1.6 copy-start.17
  123.9 2.8 copy-start.7
  123.9 2.8 copy-start.8
  124.0 2.8 copy-start.22
  124.0 2.8 copy-start.25
  124.0 4.1 copy-start.15
  124.0 4.1 copy-start.31
  124.0 4.1 copy-start.32
  124.0 4.1 copy-start.33
  124.0 4.1 copy-start.34
  124.0 4.1 copy-start.41
  126.8 1.8 copy-start.42
  128.0 0.8 copy-start.43
  128.1 1.2 copy-start.12
  128.8 1.7 copy-start.9
  130.5 1.8 copy-start.26
  130.5 1.8 copy-start.11
  130.5 4.2 %copy-start.30 = (s32[256,3]{0,1:T(4,128)S(1)}, s32[256,3]{0,1:T(4,128)}, u32[]{:S(2)}) copy-start(s32[256,3]{0,1:T(4,128)} %param.51) | copy-start | bytes 9220
  132.2 70.8 %copy-start.13 = (bf16[256,2048]{1,0:T(8,128)(2,1)S(1)}, bf16[256,2048]{1,0:T(8,128)(2,1)}, u32[]{:S(2)}) copy-start(bf16[256,2048]{1,0:T(8,128)(2,1)} %param.31) | copy-start | bytes 3145732
  132.2 159.8 %all-gather.7.cloned.1.call-start = ((), (), s32[]{:S(2)}) async-start(), calls=%async_computation.4 | async-start | bytes 5242880 | tf_op jit(solution)/shard_map/all_gather | solution.py:289
  204.6 1.4 copy-start.3
  241.4 115.9 %reduce-scatter.2.cloned.1.call-start = ((), (), s32[]{:S(2)}) async-start(), calls=%async_computation.5 | async-start | bytes 5242880 | tf_op jit(solution)/shard_map/reduce_scatter | solution.py:299
  291.9 5.3 %copy-start.44 = (bf16[1024,2048]{1,0:T(8,128)(2,1)S(1)}, bf16[1024,2048]{1,0:T(8,128)(2,1)}, u32[]{:S(2)}) copy-start(bf16[1024,2048]{1,0:T(8,128)(2,1)} %all-gather.7.cloned.1.call-done) | copy-start | bytes 12582916
  291.9 5.4 %copy-start.45 = (bf16[1,2048,512]{2,1,0:T(8,128)(2,1)S(1)}, bf16[1,2048,512]{2,1,0:T(8,128)(2,1)}, u32[]{:S(2)}) copy-start(bf16[1,2048,512]{2,1,0:T(8,128)(2,1)} %param.53) | copy-start | bytes 6291460
  304.5 57.3 %copy-start.39 = (f32[256,3]{0,1:T(4,128)S(1)}, f32[256,3]{0,1:T(4,128)}, u32[]{:S(2)}) copy-start(f32[256,3]{0,1:T(4,128)} %param.52) | copy-start | bytes 9220
  357.3 31.2 %all-to-all-start.1 = ((bf16[8,128,512]{2,1,0:T(8,128)(2,1)}), bf16[8,128,512]{2,1,0:T(8,128)(2,1)S(1)}, u32[]{:S(2)}, u32[]{:S(2)}) async-start(bf16[8,128,512]{2,1,0:T(8,128)(2,1)} %reduce-scatter.2.cloned.1.call-done), calls=%async_computation.2 | async-start | bytes 2097152 | tf_op jit(solution)/shard_map/all_to_all | solution.py:305
Sparse Core Ops, SparseCore 0:
  87.0 23.1 all-gather.8
  132.3 70.6 all-reduce.4
  241.5 50.3 all-gather.6
  304.7 52.5 reduce-scatter.1
where the time goes:
time: 409 us; the launch traced here: 407 us
  waiting for transfers between devices  190 us (46%)
  blocking collectives  62 us (15%)
  local copies, waits for them, and re-layouts  56.8 us (14%)
  other arithmetic  33.6 us (8%)
  matrix products  31.5 us (8%)
  starting transfers between devices  18 us (4%)
  between operations  14.6 us (4%)
    psum x1, waiting for transfers between devices, local(): mixed = lax.psum(partial_mix.astype(jnp.bfloat16), 'tp').astype(jnp.float32)  60.3 us
    reduce_scatter x1, waiting for transfers between devices, local(): lax.psum_scatter(partial_out.reshape(experts, capacity, -1).astype(jnp.bf...  52.7 us
    all_gather x1, waiting for transfers between devices, local(): piece = lax.all_gather(slot_parts, 'tp', axis=1, tiled=True)  50.3 us
    all_to_all x1, blocking collectives, local(): lax.all_to_all(outgoing.reshape(experts, capacity, column_width), 'sp', s...  31.1 us
    all_to_all x1, waiting for transfers between devices, local(): lax.all_to_all(summed, 'sp', split_axis=0, concat_axis=0, tiled=True)  26.4 us
    all_gather x1, blocking collectives, entering_2(): lax.all_gather(a.astype(kind), axis)  17.4 us
    unnamed x1, blocking collectives  13.6 us
    ppermute x4, starting transfers between devices, passed_along(): return lax.ppermute(block, axis, route)  13.1 us
  transfers between devices with their start and end apart: 9, of which 4 were waited for; matrix products, arithmetic and copies ran while one was open for 18% of the time, Pallas kernels for 0%

commit v1 on v0

v1 whole, which is shorter than its diff:
```python
import functools

import jax
import jax.numpy as jnp
from jax import lax
from jax.experimental import pallas as pl
from jax.experimental.pallas import tpu as pltpu
from jax.sharding import PartitionSpec as P

HEADS = 16
NARROW_HEAD_DIM = 64
WIDE_HEAD_DIM = 128
GROUPS = 4
STATE = 128
LANES = 128
CORES = 2

NORM_EPS = 1e-06
CLAMP_LIMIT = 7.0
SIGMOID_SCALE = 1.702
EXACT = lax.Precision.HIGHEST
F32 = jnp.float32
BF16 = jnp.bfloat16
VMEM = pl.BlockSpec(memory_space=pltpu.VMEM)
SMEM = pl.BlockSpec(memory_space=pltpu.SMEM)
ANY = pl.BlockSpec(memory_space=pl.ANY)


def dot(a, b, ca=1, cb=0, precision=None):
    return lax.dot_general(
        a, b, (((ca,), (cb,)), ((), ())), precision=precision, preferred_element_type=F32
    )


def iota(shape, dim):
    return lax.broadcasted_iota(jnp.int32, shape, dim)


def round_up(n, m):
    return (n + m - 1) // m * m


def silu(x):
    return x / (1.0 + jnp.exp(-x))


def call(body, outs, ins, scratch=(), flops=0, limit=56):
    single = not isinstance(outs, (list, tuple))
    outs = [outs] if single else list(outs)
    specs = [spec for spec, _ in ins]
    args = [a for _, a in ins]
    moved = sum(a.size * a.dtype.itemsize for a in args) + sum(
        o.size * o.dtype.itemsize for o in outs
    )
    res = pl.pallas_call(
        body,
        out_shape=outs,
        in_specs=specs,
        out_specs=[VMEM] * len(outs),
        scratch_shapes=list(scratch),
        compiler_params=pltpu.CompilerParams(vmem_limit_bytes=limit * 2**20),
        cost_estimate=pl.CostEstimate(
            flops=int(flops), bytes_accessed=int(moved), transcendentals=0
        ),
    )(*args)
    return res[0] if single else res


def sds(shape, dtype):
    return jax.ShapeDtypeStruct(shape, dtype)


class Heads:
    def __init__(self, count, length):
        self.count = count
        self.length = length
        self.narrow = count * NARROW_HEAD_DIM
        self.narrow_pad = round_up(self.narrow, LANES)
        self.wide = count * WIDE_HEAD_DIM
        self.width = self.narrow_pad + self.wide
        self.rows = round_up(2 * count, 8)
        per = LANES // NARROW_HEAD_DIM
        self.blocks = []
        for b in range(self.narrow_pad // LANES):
            members = []
            for h in range(b * per, min((b + 1) * per, count)):
                members.append((h, (h - b * per) * NARROW_HEAD_DIM))
            self.blocks.append((b * LANES, members))
        for h in range(count):
            self.blocks.append((self.narrow_pad + h * WIDE_HEAD_DIM, [(count + h, None)]))

    def spread(self):
        col = iota((self.rows, self.width), 1)
        row = iota((self.rows, self.width), 0)
        narrow = jnp.where(col < self.narrow, col // NARROW_HEAD_DIM, -1)
        wide = self.count + (col - self.narrow_pad) // WIDE_HEAD_DIM
        return (jnp.where(col < self.narrow_pad, narrow, wide) == row).astype(F32)

    def member(self, block, lane):
        if lane is None:
            return block
        at = iota(block.shape, 1)
        return jnp.where((at >= lane) & (at < lane + NARROW_HEAD_DIM), block, 0.0)


def upper(n):
    return (iota((n, n), 0) <= iota((n, n), 1)).astype(F32)


def mix_body(hd, rim_at, c_ref, nar, wid, key, qry, rim, tn, tw, tk, tq, a_t, step_t,
             x_out, b_out, c_out, keep, send, pad, states):
    length = hd.length
    x_out[...] = jnp.zeros(x_out.shape, F32)

    def conv(src, taps, at):
        width = src.shape[1]
        pad[0:8, :width] = rim[:, at : at + width].astype(F32)
        pad[8 : 8 + length, :width] = src[...].astype(F32)
        count = taps.shape[0]
        acc = jnp.zeros((length, width), F32)
        for j in range(count):
            acc = acc + taps[j : j + 1, :] * pad[9 - count + j : 9 - count + j + length, :width]
        return silu(acc)

    x_out[:, : hd.narrow] = conv(nar, tn, rim_at[0])
    x_out[:, hd.narrow_pad :] = conv(wid, tw, rim_at[1])
    keys = conv(key, tk, rim_at[2])
    b_out[...] = keys.astype(BF16)
    c_out[...] = conv(qry, tq, rim_at[3]).astype(BF16)
    cum = dot(a_t[...], upper(length), precision=EXACT)
    total = cum[:, length - 1 : length]
    weight = jnp.exp(total - cum) * step_t[...]
    keys_t = keys.T
    for at, members in hd.blocks:
        block = x_out[:, at : at + LANES]
        acc = jnp.zeros((STATE, LANES), F32)
        for h, lane in members:
            acc = acc + dot(
                (keys_t * weight[h : h + 1, :]).astype(BF16), hd.member(block, lane).astype(BF16)
            )
        states[:, at : at + LANES] = acc
    spread = jnp.sum(hd.spread() * total, axis=0, keepdims=True)
    high = spread.astype(BF16).astype(F32)
    row = iota((16, hd.width), 0)
    tail = jnp.where(row == 0, high, jnp.where(row == 1, spread - high, 0.0)).astype(BF16)
    half = STATE // CORES
    core = c_ref[0]
    mine = pl.multiple_of(core * half, half)
    other = pl.multiple_of((1 - core) * half, half)
    keep[0:half, :] = states[pl.ds(mine, half), :].astype(BF16)
    send[0:half, :] = states[pl.ds(other, half), :].astype(BF16)
    keep[half:, :] = tail
    send[half:, :] = tail


def inner_body(hd, x, b, c, a_t, step_t, direct, y_out):
    length = hd.length
    cum = dot(a_t[...], upper(length), precision=EXACT)
    lower = (iota((length, length), 0) >= iota((length, length), 1)).astype(F32)
    cum_col = dot(lower, a_t[...], 1, 1, precision=EXACT)
    causal = iota((length, length), 0) >= iota((length, length), 1)
    scores = dot(c[...], b[...], 1, 1)
    skip = jnp.sum(hd.spread() * direct[...], axis=0, keepdims=True)
    for at, members in hd.blocks:
        block = x[:, at : at + LANES]
        acc = skip[:, at : at + LANES] * block
        for h, lane in members:
            gap = jnp.where(causal, cum_col[:, h : h + 1] - cum[h : h + 1, :], -1e30)
            m = scores * jnp.exp(gap) * step_t[h : h + 1, :]
            acc = acc + dot(m.astype(BF16), hd.member(block, lane).astype(BF16))
        y_out[:, at : at + LANES] = acc


def project_body(hd, tp, s_ref, y, c, own, got, a_t, gate_n, gate_w, gain_n, gain_w, rows_n, rows_w, *rest):
    outs, (carry, normed) = rest[:tp], rest[tp:]
    length = hd.length
    half = STATE // CORES
    core = s_ref[0]
    place = s_ref[1]
    carry[pl.ds(pl.multiple_of(core * half, half), half), :] = own[...].astype(F32)
    carry[pl.ds(pl.multiple_of((1 - core) * half, half), half), :] = got[...].astype(F32)
    lower = (iota((length, length), 0) >= iota((length, length), 1)).astype(F32)
    cum_col = dot(lower, a_t[...], 1, 1, precision=EXACT)
    spread = hd.spread()
    decay = dot(jnp.exp(cum_col), spread, precision=EXACT)
    total = y[...] + decay * dot(c[...], carry[...].astype(BF16))

    def finish(part, gate, gain, dim):
        part = part * silu(gate[...].astype(F32))
        width = part.shape[1]
        col = iota((width, LANES), 0) // dim
        pick = (col == iota((width, LANES), 1)).astype(F32)
        mean = dot(part * part, pick, precision=EXACT) * (1.0 / dim)
        scale = dot(lax.rsqrt(mean + NORM_EPS), pick, 1, 1, precision=EXACT)
        return (part * scale * gain[...]).astype(BF16)

    out_n = finish(total[:, : hd.narrow], gate_n, gain_n, NARROW_HEAD_DIM)
    out_w = finish(total[:, hd.narrow_pad :], gate_w, gain_w, WIDE_HEAD_DIM)
    width = outs[0].shape[1]
    for d in range(tp):
        at = pl.multiple_of((place ^ d) * width, LANES)
        part = dot(out_n, rows_n[:, pl.ds(at, width)]) + dot(out_w, rows_w[:, pl.ds(at, width)])
        outs[d][...] = part.astype(BF16)


def hidden_body(tp, s_ref, resid, gain, *rest):
    parts, (hidden_out, pay_out) = rest[:tp], rest[tp:]
    length, width = parts[0].shape
    at = pl.multiple_of(s_ref[1] * width, LANES)
    hidden = resid[:, pl.ds(at, width)].astype(F32)
    total = parts[0][...].astype(F32)
    for part in parts[1:]:
        total = total + part[...].astype(F32)
    hidden = hidden + total
    hidden_out[...] = hidden
    pay_out[0:length, :] = (hidden * gain[:, pl.ds(at, width)]).astype(BF16)
    squares = dot(jnp.ones((8, width), F32), hidden * hidden, 1, 1, precision=EXACT)
    pay_out[length:, :] = jnp.zeros((pay_out.shape[0] - length, width), BF16)
    step = min(length, width)
    for i in range(length // step):
        piece = squares[0:1, i * step : (i + 1) * step]
        high = piece.astype(BF16)
        pay_out[length + i : length + i + 1, 0:step] = high
        pay_out[length + 8 + i : length + 9 + i, 0:step] = (piece - high.astype(F32)).astype(BF16)


def hits_of(rt, expert, picks):
    hit = jnp.zeros((1, rt.shape[1]), F32)
    load = jnp.zeros((1, rt.shape[1]), F32)
    for k in range(picks):
        match = (rt[k : k + 1, :] == expert).astype(F32)
        hit = hit + match
        load = load + match * rt[picks + k : picks + k + 1, :]
    return hit, load


def slots_of(hit, cap):
    length = hit.shape[1]
    before = (iota((length, length), 0) < iota((length, length), 1)).astype(BF16)
    rank = dot(jnp.broadcast_to(hit, (8, length)).astype(BF16), before)[0:1, :]
    slot = iota((cap, length), 0).astype(F32)
    return jnp.where((rank == slot) & (hit > 0.5), 1.0, 0.0)


def select_body(n, cap, picks, s_ref, *rest):
    pays, rts, outs = rest[:n], rest[n : 2 * n], rest[2 * n :]
    length = rts[0].shape[1]
    width = pays[0].shape[1]
    step = min(length, width)
    for out in outs:
        out[n * cap :, :] = jnp.zeros((out.shape[0] - n * cap, width), BF16)
    for i in range(n):
        rt = rts[i][...]
        block = pays[i][0:length, :]
        pieces = []
        for j in range(length // step):
            high = pays[i][length + j : length + j + 1, 0:step].astype(F32)
            low = pays[i][length + 8 + j : length + 9 + j, 0:step].astype(F32)
            pieces.append(high + low)
        squares = pieces[0] if len(pieces) == 1 else jnp.concatenate(pieces, axis=1)
        squares = jnp.broadcast_to(squares, (8, length))
        for which, out in enumerate(outs):
            hit, _ = hits_of(rt, s_ref[2 + which].astype(F32), picks)
            onehot = slots_of(hit, cap)
            out[i * cap : (i + 1) * cap, :] = dot(onehot.astype(BF16), block).astype(BF16)
            ssq = dot(squares, onehot, 1, 1, precision=EXACT)[0:1, :]
            high = ssq.astype(BF16)
            out[n * cap + i : n * cap + i + 1, 0:cap] = high
            out[n * cap + n + i : n * cap + n + i + 1, 0:cap] = (ssq - high.astype(F32)).astype(BF16)


def expert_body(tp, n, cap, model, s_ref, *rest):
    xs, weights, outs = rest[:tp], rest[tp : tp + 9], rest[tp + 9 : 2 * tp + 9]
    bufs, sems = rest[2 * tp + 9 : 2 * tp + 15], rest[2 * tp + 15]
    own, first, second = weights[0:3], weights[3:6], weights[6:9]
    native = s_ref[4]

    def start(source, q):
        for m in range(3):
            pltpu.make_async_copy(source[m], bufs[3 * q + m], sems.at[3 * q + m]).start()

    @pl.when(native == 1)
    def _():
        start(own, 0)
        start(first, 1)

    @pl.when(native == 0)
    def _():
        start(first, 0)
        start(second, 1)

    def arrive(q, m):
        pltpu.make_async_copy(own[m], bufs[3 * q + m], sems.at[3 * q + m]).wait()

    place = s_ref[1]
    width = xs[0].shape[1]
    eye = (iota((cap, cap), 0) == iota((cap, cap), 1)).astype(F32)
    scales = []
    for i in range(n):
        ssq = jnp.zeros((1, cap), F32)
        for x in xs:
            ssq = ssq + x[n * cap + i : n * cap + i + 1, 0:cap].astype(F32)
            ssq = ssq + x[n * cap + n + i : n * cap + n + i + 1, 0:cap].astype(F32)
        col = dot(eye, jnp.broadcast_to(ssq, (8, cap)), 1, 1, precision=EXACT)[:, 0:1]
        scales.append(lax.rsqrt(col * (1.0 / model) + NORM_EPS))
    scale = jnp.concatenate(scales, axis=0) if n > 1 else scales[0]

    def product(buf):
        acc = None
        for d in range(tp):
            at = pl.multiple_of((place ^ d) * width, LANES)
            part = dot(xs[d][0 : n * cap, :], buf[pl.ds(at, width), :])
            acc = part if acc is None else acc + part
        return acc * scale

    acts = []
    for q in range(CORES):
        arrive(q, 0)
        gate = jnp.minimum(product(bufs[3 * q]), CLAMP_LIMIT)
        arrive(q, 1)
        up = jnp.clip(product(bufs[3 * q + 1]), -CLAMP_LIMIT, CLAMP_LIMIT)
        act = (up + 1.0) * gate / (1.0 + jnp.exp(-SIGMOID_SCALE * gate))
        acts.append(act.astype(BF16))
    for q in range(CORES):
        arrive(q, 2)
    for d in range(tp):
        at = pl.multiple_of((place ^ d) * width, LANES)
        part = None
        for q in range(CORES):
            one = dot(acts[q], bufs[3 * q + 2][:, pl.ds(at, width)])
            part = one if part is None else part + one
        outs[d][...] = part.astype(BF16)


def combine_body(tp, n, cap, picks, s_ref, *rest):
    parts, rts, outs = rest[:tp], rest[tp : tp + n], rest[tp + n :]
    for i in range(n):
        rt = rts[i][...]
        rows = slice(i * cap, (i + 1) * cap)
        total = None
        for which in range(2):
            group = parts[: tp // 2] if which == 0 else parts[tp // 2 :]
            value = group[0][rows, :].astype(F32)
            for part in group[1:]:
                value = value + part[rows, :].astype(F32)
            hit, load = hits_of(rt, s_ref[2 + which].astype(F32), picks)
            placed = slots_of(hit, cap) * load
            one = dot(placed, value, 0, 0, precision=EXACT)
            total = one if total is None else total + one
        outs[i][...] = total.astype(BF16)


def local(
    resid,
    narrow_head_input,
    wide_head_input,
    key_group_input,
    query_group_input,
    narrow_output_gate,
    wide_output_gate,
    step_input_rows,
    head_decay_logarithm,
    position_log_decay,
    direct_input_weight,
    narrow_conv_taps,
    wide_conv_taps,
    key_conv_taps,
    query_conv_taps,
    narrow_norm_gain,
    wide_norm_gain,
    narrow_output_rows,
    wide_output_rows,
    feedforward_norm_gain,
    routes,
    routing_weight_values,
    expert_gate_matrix,
    expert_up_matrix,
    expert_down_matrix,
):
    sp, tp = lax.axis_size("sp"), lax.axis_size("tp")
    chips = sp // CORES
    sp_at, tp_at = lax.axis_index("sp"), lax.axis_index("tp")
    chip, core = sp_at // CORES, sp_at % CORES
    side = tp_at // (tp // 2)
    native = (side == core).astype(jnp.int32)
    length, model = resid.shape
    width = model // tp
    hd = Heads(narrow_head_input.shape[1] // NARROW_HEAD_DIM, length)
    picks = routes.shape[1]
    cap = 4 * length * picks // (3 * sp)
    scalars = jnp.stack(
        [core, tp_at, CORES * chip + side, CORES * chip + 1 - side, native]
    ).astype(jnp.int32)

    def shift(x, by):
        return lax.ppermute(x, "sp", [(i, i + by) for i in range(sp - by)])

    def flip(x, axis, size, bits):
        return lax.ppermute(x, axis, [(i, i ^ bits) for i in range(size)])

    def over_z(x, d):
        return flip(x, "sp", sp, CORES * d)

    def over_tp(x, d):
        return flip(x, "tp", tp, d)

    def to_partner(x):
        return flip(x, "sp", sp, 1)

    group = tp_at * hd.count // (HEADS // GROUPS)
    key_in = lax.dynamic_slice_in_dim(key_group_input, group * STATE, STATE, 1)
    query_in = lax.dynamic_slice_in_dim(query_group_input, group * STATE, STATE, 1)
    key_taps = lax.dynamic_slice_in_dim(key_conv_taps, group * STATE, STATE, 1)
    query_taps = lax.dynamic_slice_in_dim(query_conv_taps, group * STATE, STATE, 1)
    pieces, rim_at, at = [], [], 0
    for src in (narrow_head_input, wide_head_input, key_in, query_in):
        last = src[length - 8 :]
        extra = round_up(last.shape[1], LANES) - last.shape[1]
        pieces.append(jnp.pad(last, ((0, 0), (0, extra))) if extra else last)
        rim_at.append(at)
        at += last.shape[1] + extra
    rim = shift(jnp.concatenate(pieces, axis=1), 1)

    mats = (expert_gate_matrix[0], expert_up_matrix[0], expert_down_matrix[0])
    swap, share = [], []
    for s in range(sp):
        for t in range(tp):
            if t // (tp // 2) == s % CORES:
                swap.append((s * tp + t, (s ^ 1) * tp + t))
                share.append((s * tp + t, (s ^ 1) * tp + t))
            else:
                swap.append((s * tp + t, s * tp + (t ^ (tp // 2))))
    first = [lax.ppermute(m, ("sp", "tp"), swap) for m in mats]
    second = [lax.ppermute(m, ("sp", "tp"), share) for m in first]

    table = jnp.concatenate([routes.T.astype(F32), routing_weight_values.T], axis=0)
    table = jnp.pad(table, ((0, round_up(2 * picks, 8) - 2 * picks), (0, 0)))
    tables = [table] + [over_z(table, d) for d in range(1, chips)]

    def by_head(a):
        rows = jnp.transpose(a, (1, 2, 0)).reshape(2 * hd.count, -1)
        return jnp.pad(rows, ((0, hd.rows - 2 * hd.count), (0, 0)))

    step_t = jax.nn.softplus(step_input_rows.astype(F32))
    decay_t = -jnp.exp(head_decay_logarithm)[None] * step_t + position_log_decay
    step_t, decay_t = by_head(step_t), by_head(decay_t)
    direct = by_head(direct_input_weight[None])

    wide_cols = max(hd.narrow, hd.wide, STATE)
    half = STATE // CORES
    x, b, c, keep, send = call(
        functools.partial(mix_body, hd, tuple(rim_at)),
        [
            sds((length, hd.width), F32),
            sds((length, STATE), BF16),
            sds((length, STATE), BF16),
            sds((half + 16, hd.width), BF16),
            sds((half + 16, hd.width), BF16),
        ],
        [
            (SMEM, scalars),
            (VMEM, narrow_head_input),
            (VMEM, wide_head_input),
            (VMEM, key_in),
            (VMEM, query_in),
            (VMEM, rim),
            (VMEM, narrow_conv_taps),
            (VMEM, wide_conv_taps),
            (VMEM, key_taps),
            (VMEM, query_taps),
            (VMEM, decay_t),
            (VMEM, step_t),
        ],
        [pltpu.VMEM((length + 8, wide_cols), F32), pltpu.VMEM((STATE, hd.width), F32)],
        flops=2e9,
    )

    got = to_partner(send)
    early = jnp.where(core == 0, keep, got).astype(F32)
    late = jnp.where(core == 0, got, keep).astype(F32)

    def parts_of(p):
        return p[:half], p[half : half + 1] + p[half + 1 : half + 2]

    state_0, total_0 = parts_of(early)
    state_1, total_1 = parts_of(late)
    both = total_0 + total_1
    high = both.astype(BF16)
    low = (both - high.astype(F32)).astype(BF16)
    chip_pay = jnp.concatenate(
        [
            (jnp.exp(total_1) * state_0 + state_1).astype(BF16),
            high,
            low,
            jnp.zeros((14, hd.width), BF16),
        ],
        axis=0,
    )
    arrived = [shift(chip_pay, CORES * d) for d in range(1, chips)]

    y = call(
        functools.partial(inner_body, hd),
        sds((length, hd.width), F32),
        [(VMEM, x), (VMEM, b), (VMEM, c), (VMEM, decay_t), (VMEM, step_t), (VMEM, direct)],
        flops=4e9,
    )

    carry = jnp.zeros((half, hd.width), F32)
    passed = jnp.zeros((1, hd.width), F32)
    for one in arrived:
        state, total = parts_of(one.astype(F32))
        carry = carry + jnp.exp(passed) * state
        passed = passed + total
    carry_0 = carry
    carry_1 = jnp.exp(total_0) * carry + state_0
    own_carry = jnp.where(core == 0, carry_0, carry_1).astype(BF16)
    other_carry = to_partner(jnp.where(core == 0, carry_1, carry_0).astype(BF16))

    parts = call(
        functools.partial(project_body, hd, tp),
        [sds((length, width), BF16)] * tp,
        [
            (SMEM, scalars),
            (VMEM, y),
            (VMEM, c),
            (VMEM, own_carry),
            (VMEM, other_carry),
            (VMEM, decay_t),
            (VMEM, narrow_output_gate),
            (VMEM, wide_output_gate),
            (VMEM, narrow_norm_gain[None]),
            (VMEM, wide_norm_gain[None]),
            (VMEM, narrow_output_rows),
            (VMEM, wide_output_rows),
        ],
        [pltpu.VMEM((STATE, hd.width), F32), pltpu.VMEM((8, LANES), F32)],
        flops=2e9,
    )
    parts = [parts[0]] + [over_tp(parts[d], d) for d in range(1, tp)]

    hidden, pay = call(
        functools.partial(hidden_body, tp),
        [sds((length, width), F32), sds((length + 16, width), BF16)],
        [(SMEM, scalars), (VMEM, resid), (VMEM, feedforward_norm_gain[None])]
        + [(VMEM, p) for p in parts],
        flops=1e9,
    )
    pays = [pay] + [over_z(pay, d) for d in range(1, chips)]

    groups = 2
    per = chips // groups
    out = hidden
    for g in range(groups):
        members = range(g * per, (g + 1) * per)
        n = len(members)
        rows = n * cap + round_up(2 * n, 16)
        same, other = call(
            functools.partial(select_body, n, cap, picks),
            [sds((rows, width), BF16)] * 2,
            [(SMEM, scalars)]
            + [(VMEM, pays[d]) for d in members]
            + [(VMEM, tables[d]) for d in members],
            flops=1e9,
        )
        xs = [same] + [over_tp(same if d < tp // 2 else other, d) for d in range(1, tp)]
        ff = mats[0].shape[1]
        results = call(
            functools.partial(expert_body, tp, n, cap, model),
            [sds((n * cap, width), BF16)] * tp,
            [(SMEM, scalars)]
            + [(VMEM, a) for a in xs]
            + [(ANY, a) for a in (*mats, *first, *second)],
            [pltpu.VMEM(m.shape, BF16) for m in (*mats, *mats)] + [pltpu.SemaphoreType.DMA((6,))],
            flops=12 * n * cap * model * ff,
        )
        results = [results[0]] + [over_tp(results[d], d) for d in range(1, tp)]
        sums = call(
            functools.partial(combine_body, tp, n, cap, picks),
            [sds((length, width), BF16)] * n,
            [(SMEM, scalars)]
            + [(VMEM, a) for a in results]
            + [(VMEM, tables[d]) for d in members],
            flops=1e9,
        )
        for d, one in zip(members, sums):
            out = out + (over_z(one, d) if d else one).astype(F32)
    return out.astype(BF16)


def solution(mesh):
    return jax.shard_map(
        local,
        mesh=mesh,
        in_specs=(
            P("sp", None),
            P("sp", "tp"),
            P("sp", "tp"),
            P("sp", None),
            P("sp", None),
            P("sp", "tp"),
            P("sp", "tp"),
            P("sp", None, "tp"),
            P(None, "tp"),
            P("sp", None, "tp"),
            P(None, "tp"),
            P(None, "tp"),
            P(None, "tp"),
            P(),
            P(),
            P("tp"),
            P("tp"),
            P("tp", None),
            P("tp", None),
            P(),
            P("sp", None),
            P("sp", None),
            P("sp", None, "tp"),
            P("sp", None, "tp"),
            P("sp", "tp", None),
        ),
        out_specs=P("sp", "tp"),
        check_vma=False,
    )
```

time: 409 us -> 233 us (0.57)
  waiting for transfers between devices: 190 us -> 91.9 us
  blocking collectives: 62 us -> 0 us
  starting transfers between devices: 18 us -> 70.8 us
  Pallas kernels: 0 us -> 47.7 us
  local copies, waits for them, and re-layouts: 56.8 us -> 15.3 us
  matrix products: 31.5 us -> 0 us
  other arithmetic: 33.6 us -> 4.28 us
  between operations: 14.6 us -> 0.36 us
    ppermute x4 -> x36, waiting for transfers between devices: 0.01 us -> 91.9 us  [the longest x26 55.5 us: flip(): return lax.ppermute(x, axis, [(i, i ^ bits) for i in range(size)])]
    psum x1 -> x0, waiting for transfers between devices: 60.3 us -> none  [local(): mixed = lax.psum(partial_mix.astype(jnp.bfloat16), 'tp').astype(jnp.float32)]
    ppermute x4 -> x36, starting transfers between devices: 13.1 us -> 70.8 us  [the longest x26 43.6 us: flip(): return lax.ppermute(x, axis, [(i, i ^ bits) for i in range(size)])]
    reduce_scatter x1 -> x0, waiting for transfers between devices: 52.7 us -> none  [local(): lax.psum_scatter(partial_out.reshape(experts, capacity, -1).astype(jnp.bf...]
    all_gather x2 -> x0, waiting for transfers between devices: 50.3 us -> none  [the longest x1 50.3 us: local(): piece = lax.all_gather(slot_parts, 'tp', axis=1, tiled=True)]
    pallas_call x0 -> x10, Pallas kernels: none -> 47.7 us  [call(): pl.pallas_call(body, out_shape=outs, in_specs=specs, out_specs=[VMEM] * l...]
    dot_general x14 -> x0, matrix products: 31.5 us -> none  [the longest x2 5.99 us: pick_groups(): return jnp.einsum('sgn,hg->shn', grouped, chooser, precision=FULL_PRECISION)]
    all_to_all x1 -> x0, blocking collectives: 31.1 us -> none  [local(): lax.all_to_all(outgoing.reshape(experts, capacity, column_width), 'sp', s...]
  transfers between devices with their start and end apart: 9 -> 36, of which waited for: 4 -> 13; matrix products, arithmetic and copies ran while one was open for 18% -> 4% of each run, Pallas kernels for 0% -> 21%
where the time goes in v1:
time: 233 us; the launch traced here: 230 us
  waiting for transfers between devices  91.9 us (39%)
  starting transfers between devices  70.8 us (30%)
  Pallas kernels  47.7 us (20%)
  local copies, waits for them, and re-layouts  15.3 us (7%)
  other arithmetic  4.28 us (2%)
    ppermute x26, waiting for transfers between devices, flip(): return lax.ppermute(x, axis, [(i, i ^ bits) for i in range(size)])  55.5 us
    pallas_call x10, Pallas kernels, call(): pl.pallas_call(body, out_shape=outs, in_specs=specs, out_specs=[VMEM] * l...  47.7 us
    ppermute x26, starting transfers between devices, flip(): return lax.ppermute(x, axis, [(i, i ^ bits) for i in range(size)])  43.6 us
    ppermute x3, waiting for transfers between devices, local(): first = [lax.ppermute(m, ('sp', 'tp'), swap) for m in mats]  34.8 us
    ppermute x4, starting transfers between devices, shift(): return lax.ppermute(x, 'sp', [(i, i + by) for i in range(sp - by)])  14.4 us
    ppermute x3, starting transfers between devices, local(): second = [lax.ppermute(m, ('sp', 'tp'), share) for m in first]  8.95 us
    unnamed x64, local copies, waits for them, and re-layouts  7.16 us
  transfers between devices with their start and end apart: 36, of which 13 were waited for; matrix products, arithmetic and copies ran while one was open for 4% of the time, Pallas kernels for 21%

profile of v1, /device:TPU:0, one launch (start us, length us, event | category | flops | bytes accessed | tf_op | source)
XLA Modules:
  0.0 230.4 jit_solution(6370461567880903877)
XLA Ops:
  0.0 0.7 dynamic-slice
  0.7 0.7 dynamic-slice.1
  1.4 0.7 slice.55
  2.1 0.7 slice.54
  2.8 2.4 %collective-permute-start = (bf16[8,1024]{1,0:T(8,128)(2,1)S(1)}, bf16[8,1024]{1,0:T(8,128)(2,1)S(1)}, u32[]{:S(2)}, u32[]{:S(2)}) collective-permute-start(bf16[8,1024]{1,0:T(8,128)(2,1)S(1)} %pad_maximum_fusion), channel_id=1, source_target_pairs={{0,4},{4,8},{8,12},{12,16},{16,20},{20,24},{24,28},{1,5},{5,9},{9,... | collective-permute-start | bytes 49160 | tf_op jit(solution)/shard_map/ppermute | solution.py:396
  5.2 2.7 %collective-permute-start.14 = (bf16[2048,512]{1,0:T(8,128)(2,1)}, bf16[2048,512]{1,0:T(8,128)(2,1)S(1)}, u32[]{:S(2)}, u32[]{:S(2)}) collective-permute-start(bf16[2048,512]{1,0:T(8,128)(2,1)} %bitcast.18), channel_id=1, source_target_pairs={{0,4},{1,5},{2,0},{3,1},{4,6},{5,7},{6,2},{7,3},{8,12},{9,13},{10,... | collective-permute-start | bytes 6291464 | tf_op jit(solution)/shard_map/ppermute | solution.py:433
  7.8 1.2 collective-permute-start.15
  9.1 1.5 constant_dynamic-slice_fusion.2
  10.6 0.7 exponential_negate_fusion
  11.3 0.8 fusion.8
  12.1 1.3 constant_dynamic-slice_fusion
  15.8 3.2 %shard_map.235 = (f32[256,768]{1,0:T(8,128)}, bf16[256,128]{1,0:T(8,128)(2,1)}, bf16[256,128]{1,0:T(8,128)(2,1)}, bf16[80,768]{1,0:T(8,128)(2,1)}, bf16[80,768]{1,0:T(8,128)(2,1)}) custom-call(s32[5]{0:T(128)} %stack.27.c_ref.s_ref, bf16[256,256]{1,0:T(8,128)(2,1)} %nar.1, bf16[256,512]{1,0:T(8,128)(2,1)} %wid.1, bf16[256,128]{1,0:T(8,128)(2,1)} %get-tuple-element.76.key, ...), custom_call_target="tpu_custom_call" | custom-call | flops 2000000000 | bytes 1736724 | tf_op jit(solution)/shard_map/pallas_call | solution.py:55
  19.1 1.4 collective-permute-done.1
  20.6 0.9 select_convert_fusion.3
  21.7 3.5 %collective-permute-start.2 = (bf16[80,768]{1,0:T(8,128)(2,1)S(1)}, bf16[80,768]{1,0:T(8,128)(2,1)S(1)}, u32[]{:S(2)}, u32[]{:S(2)}) collective-permute-start(bf16[80,768]{1,0:T(8,128)(2,1)S(1)} %maximum_maximum_fusion), channel_id=1, source_target_pairs={{0,8},{4,12},{8,16},{12,20},{16,24},{20,28},{1,9},{5,13},{9,17},{1... | collective-permute-start | bytes 368648 | tf_op jit(solution)/shard_map/ppermute | solution.py:396
  25.2 3.4 %collective-permute-start.3 = (bf16[80,768]{1,0:T(8,128)(2,1)S(1)}, bf16[80,768]{1,0:T(8,128)(2,1)S(1)}, u32[]{:S(2)}, u32[]{:S(2)}) collective-permute-start(bf16[80,768]{1,0:T(8,128)(2,1)S(1)} %maximum_maximum_fusion), channel_id=1, source_target_pairs={{0,16},{4,20},{8,24},{12,28},{1,17},{5,21},{9,25},{13,29},{2,18},{... | collective-permute-start | bytes 368648 | tf_op jit(solution)/shard_map/ppermute | solution.py:396
  28.7 5.1 %collective-permute-start.4 = (bf16[80,768]{1,0:T(8,128)(2,1)S(1)}, bf16[80,768]{1,0:T(8,128)(2,1)S(1)}, u32[]{:S(2)}, u32[]{:S(2)}) collective-permute-start(bf16[80,768]{1,0:T(8,128)(2,1)S(1)} %maximum_maximum_fusion), channel_id=1, source_target_pairs={{0,24},{4,28},{1,25},{5,29},{2,26},{6,30},{3,27},{7,31}} | collective-permute-start | bytes 368648 | tf_op jit(solution)/shard_map/ppermute | solution.py:396
  34.5 1.6 collective-permute-done.4
  36.1 0.7 select_convert_fusion
  36.9 2.5 %collective-permute-start.17 = (bf16[2048,512]{1,0:T(8,128)(2,1)S(1)}, bf16[2048,512]{1,0:T(8,128)(2,1)S(1)}, u32[]{:S(2)}, u32[]{:S(2)}) collective-permute-start(bf16[2048,512]{1,0:T(8,128)(2,1)S(1)} %collective-permute-done.14.rest_7_), channel_id=1, source_target_pairs={{0,4},{1,5},{6,2},{7,3},{8,12},{9,13},{14,10},{15,11},{16,20},{17,... | collective-permute-start | bytes 6291464 | tf_op jit(solution)/shard_map/ppermute | solution.py:434
  39.4 14.9 %collective-permute-done.15.rest_8_ = bf16[2048,512]{1,0:T(8,128)(2,1)} collective-permute-done((bf16[2048,512]{1,0:T(8,128)(2,1)}, bf16[2048,512]{1,0:T(8,128)(2,1)}, u32[]{:S(2)}, u32[]{:S(2)}) %collective-permute-start.15) | collective-permute-done | bytes 2097184 | tf_op jit(solution)/shard_map/ppermute | solution.py:433
  54.3 2.6 %collective-permute-start.18 = (bf16[2048,512]{1,0:T(8,128)(2,1)}, bf16[2048,512]{1,0:T(8,128)(2,1)S(1)}, u32[]{:S(2)}, u32[]{:S(2)}) collective-permute-start(bf16[2048,512]{1,0:T(8,128)(2,1)} %collective-permute-done.15.rest_8_), channel_id=1, source_target_pairs={{0,4},{1,5},{6,2},{7,3},{8,12},{9,13},{14,10},{15,11},{16,20},{17,... | collective-permute-start | bytes 6291464 | tf_op jit(solution)/shard_map/ppermute | solution.py:434
  56.9 19.9 %collective-permute-done.16.rest_9_ = bf16[512,2048]{1,0:T(8,128)(2,1)} collective-permute-done((bf16[512,2048]{1,0:T(8,128)(2,1)}, bf16[512,2048]{1,0:T(8,128)(2,1)}, u32[]{:S(2)}, u32[]{:S(2)}) %collective-permute-start.16) | collective-permute-done | bytes 2097184 | tf_op jit(solution)/shard_map/ppermute | solution.py:433
  76.8 3.9 %collective-permute-start.19 = (bf16[512,2048]{1,0:T(8,128)(2,1)}, bf16[512,2048]{1,0:T(8,128)(2,1)}, u32[]{:S(2)}, u32[]{:S(2)}) collective-permute-start(bf16[512,2048]{1,0:T(8,128)(2,1)} %collective-permute-done.16.rest_9_), channel_id=1, source_target_pairs={{0,4},{1,5},{6,2},{7,3},{8,12},{9,13},{14,10},{15,11},{16,20},{17,... | collective-permute-start | bytes 6291464 | tf_op jit(solution)/shard_map/ppermute | solution.py:434
  80.6 3.2 %shard_map.236.y = f32[256,768]{1,0:T(8,128)} custom-call(f32[256,768]{1,0:T(8,128)} %get-tuple-element.32.x, bf16[256,128]{1,0:T(8,128)(2,1)} %get-tuple-element.33.b, bf16[256,128]{1,0:T(8,128)(2,1)} %get-tuple-element.34.c, f32[8,256]{1,0:T(8,128)} %reshape.8.a_t, f32[8,256]{1,0:T(8,128)} %reshape.9.step_t, f32[8,1]{1,0:T(8,128)} %reshape_transpose_broadcast_in_dim.4.direct), custom_call_target="tpu_custom_call" | custom-call | flops 4000000000 | bytes 1720352 | tf_op jit(solution)/shard_map/pallas_call | solution.py:55
  84.5 7.7 %shard_map.237 = (bf16[256,512]{1,0:T(8,128)(2,1)}, bf16[256,512]{1,0:T(8,128)(2,1)}, bf16[256,512]{1,0:T(8,128)(2,1)}, bf16[256,512]{1,0:T(8,128)(2,1)}) custom-call(s32[5]{0:T(128)} %stack.27.c_ref.s_ref, f32[256,768]{1,0:T(8,128)} %shard_map.236.y, bf16[256,128]{1,0:T(8,128)(2,1)} %get-tuple-element.34.c, bf16[64,768]{1,0:T(8,128)(2,1)} %get-tuple-element.66.own, ...), custom_call_target="tpu_custom_call" | custom-call | flops 2000000000 | bytes 5647380 | tf_op jit(solution)/shard_map/pallas_call | solution.py:55
  92.2 1.5 collective-permute-start.6
  93.7 5.1 %collective-permute-done.6.rest_1_ = bf16[256,512]{1,0:T(8,128)(2,1)S(1)} collective-permute-done((bf16[256,512]{1,0:T(8,128)(2,1)}, bf16[256,512]{1,0:T(8,128)(2,1)S(1)}, u32[]{:S(2)}, u32[]{:S(2)}) %collective-permute-start.6) | collective-permute-done | bytes 262176 | tf_op jit(solution)/shard_map/ppermute | solution.py:399
  98.8 8.5 %collective-permute-done.7.rest_2_ = bf16[256,512]{1,0:T(8,128)(2,1)S(1)} collective-permute-done((bf16[256,512]{1,0:T(8,128)(2,1)}, bf16[256,512]{1,0:T(8,128)(2,1)S(1)}, u32[]{:S(2)}, u32[]{:S(2)}) %collective-permute-start.7) | collective-permute-done | bytes 262176 | tf_op jit(solution)/shard_map/ppermute | solution.py:399
  107.3 0.7 copy-done.25
  108.1 2.9 %shard_map.238 = (f32[256,512]{1,0:T(8,128)}, bf16[272,512]{1,0:T(8,128)(2,1)}) custom-call(s32[5]{0:T(128)} %stack.27.c_ref.s_ref, bf16[256,2048]{1,0:T(8,128)(2,1)} %resid.1, f32[1,2048]{1,0:T(1,128)} %bitcast.28, bf16[256,512]{1,0:T(8,128)(2,1)} %get-tuple-element.37.rest_0_, bf16[256,512]{1,0:T(8,128)(2,1)} %copy-done.24, bf16[256,512]{1,0:T(8,128)(2,1)} %copy-done.25, ...), custom_call_target="tpu_custom_call" | custom-call | flops 1000000000 | bytes 2908180 | tf_op jit(solution)/shard_map/pallas_call | solution.py:55
  111.0 1.6 collective-permute-start.9
  113.1 5.4 %collective-permute-done.10.rest_3_.rest_5_ = f32[8,256]{1,0:T(8,128)S(1)} collective-permute-done((f32[8,256]{1,0:T(8,128)S(1)}, f32[8,256]{1,0:T(8,128)S(1)}, u32[]{:S(2)}, u32[]{:S(2)}) %collective-permute-start.10) | collective-permute-done | bytes 8224 | tf_op jit(solution)/shard_map/ppermute | solution.py:399
  118.5 2.6 %collective-permute-start.26 = (f32[8,256]{1,0:T(8,128)S(1)}, f32[8,256]{1,0:T(8,128)S(1)}, u32[]{:S(2)}, u32[]{:S(2)}) collective-permute-start(f32[8,256]{1,0:T(8,128)S(1)} %select_maximum_fusion.rest_2_.rest_4_), channel_id=1, source_target_pairs={{0,16},{4,20},{8,24},{12,28},{16,0},{20,4},{24,8},{28,12},{1,17},{... | collective-permute-start | bytes 24584 | tf_op jit(solution)/shard_map/ppermute | solution.py:399
  121.2 1.9 collective-permute-done.26.rest_2_.rest_4_
  123.1 3.8 %collective-permute-start.27 = (f32[8,256]{1,0:T(8,128)S(1)}, f32[8,256]{1,0:T(8,128)S(1)}, u32[]{:S(2)}, u32[]{:S(2)}) collective-permute-start(f32[8,256]{1,0:T(8,128)S(1)} %select_maximum_fusion.rest_2_.rest_4_), channel_id=1, source_target_pairs={{0,24},{4,28},{8,16},{12,20},{16,8},{20,12},{24,0},{28,4},{1,25},{... | collective-permute-start | bytes 24584 | tf_op jit(solution)/shard_map/ppermute | solution.py:399
  126.9 1.7 collective-permute-done.27.rest_3_.rest_5_
  128.6 1.5 collective-permute-start.24
  130.2 2.4 %collective-permute-start.25 = (bf16[272,512]{1,0:T(8,128)(2,1)}, bf16[272,512]{1,0:T(8,128)(2,1)S(1)}, u32[]{:S(2)}, u32[]{:S(2)}) collective-permute-start(bf16[272,512]{1,0:T(8,128)(2,1)} %get-tuple-element.42.rest_0_), channel_id=1, source_target_pairs={{0,24},{4,28},{8,16},{12,20},{16,8},{20,12},{24,0},{28,4},{1,25},{... | collective-permute-start | bytes 835592 | tf_op jit(solution)/shard_map/ppermute | solution.py:399
  132.6 2.8 %shard_map.239 = (bf16[272,512]{1,0:T(8,128)(2,1)}, bf16[272,512]{1,0:T(8,128)(2,1)}) custom-call(s32[5]{0:T(128)} %stack.27.c_ref.s_ref, bf16[272,512]{1,0:T(8,128)(2,1)} %get-tuple-element.42.rest_0_, bf16[272,512]{1,0:T(8,128)(2,1)} %copy-done.15, f32[8,256]{1,0:T(8,128)} %copy-done.11, f32[8,256]{1,0:T(8,128)} %copy-done.31), custom_call_target="tpu_custom_call" | custom-call | flops 1000000000 | bytes 1130516 | tf_op jit(solution)/shard_map/pallas_call | solution.py:55
  135.4 11.8 %collective-permute-done.24.rest_0_ = bf16[272,512]{1,0:T(8,128)(2,1)S(1)} collective-permute-done((bf16[272,512]{1,0:T(8,128)(2,1)}, bf16[272,512]{1,0:T(8,128)(2,1)S(1)}, u32[]{:S(2)}, u32[]{:S(2)}) %collective-permute-start.24) | collective-permute-done | bytes 278560 | tf_op jit(solution)/shard_map/ppermute | solution.py:399
  147.2 1.1 collective-permute-start.11
  148.3 3.9 %collective-permute-start.12 = (bf16[272,512]{1,0:T(8,128)(2,1)}, bf16[272,512]{1,0:T(8,128)(2,1)S(1)}, u32[]{:S(2)}, u32[]{:S(2)}) collective-permute-start(bf16[272,512]{1,0:T(8,128)(2,1)} %get-tuple-element.44), channel_id=1, source_target_pairs={{0,2},{1,3},{2,0},{3,1},{4,6},{5,7},{6,4},{7,5},{8,10},{9,11},{10,... | collective-permute-start | bytes 835592 | tf_op jit(solution)/shard_map/ppermute | solution.py:399
  152.2 2.1 collective-permute-done.11.rest_1_
  154.3 5.3 %collective-permute-start.13 = (bf16[272,512]{1,0:T(8,128)(2,1)}, bf16[272,512]{1,0:T(8,128)(2,1)S(1)}, u32[]{:S(2)}, u32[]{:S(2)}) collective-permute-start(bf16[272,512]{1,0:T(8,128)(2,1)} %get-tuple-element.44), channel_id=1, source_target_pairs={{0,3},{1,2},{2,1},{3,0},{4,7},{5,6},{6,5},{7,4},{8,11},{9,10},{10,... | collective-permute-start | bytes 835592 | tf_op jit(solution)/shard_map/ppermute | solution.py:399
  159.6 2.8 %shard_map.242 = (bf16[272,512]{1,0:T(8,128)(2,1)}, bf16[272,512]{1,0:T(8,128)(2,1)}) custom-call(s32[5]{0:T(128)} %stack.27.c_ref.s_ref, bf16[272,512]{1,0:T(8,128)(2,1)} %copy-done.16, bf16[272,512]{1,0:T(8,128)(2,1)} %copy-done.17, f32[8,256]{1,0:T(8,128)} %copy-done.29, f32[8,256]{1,0:T(8,128)} %copy-done.30), custom_call_target="tpu_custom_call" | custom-call | flops 1000000000 | bytes 1130516 | tf_op jit(solution)/shard_map/pallas_call | solution.py:55
  162.5 2.7 %collective-permute-done.13.rest_3_ = bf16[272,512]{1,0:T(8,128)(2,1)S(1)} collective-permute-done((bf16[272,512]{1,0:T(8,128)(2,1)}, bf16[272,512]{1,0:T(8,128)(2,1)S(1)}, u32[]{:S(2)}, u32[]{:S(2)}) %collective-permute-start.13) | collective-permute-done | bytes 278560 | tf_op jit(solution)/shard_map/ppermute | solution.py:399
  165.3 3.3 %collective-permute-start.30 = (bf16[272,512]{1,0:T(8,128)(2,1)}, bf16[272,512]{1,0:T(8,128)(2,1)S(1)}, u32[]{:S(2)}, u32[]{:S(2)}) collective-permute-start(bf16[272,512]{1,0:T(8,128)(2,1)} %get-tuple-element.52), channel_id=1, source_target_pairs={{0,3},{1,2},{2,1},{3,0},{4,7},{5,6},{6,5},{7,4},{8,11},{9,10},{10,... | collective-permute-start | bytes 835592 | tf_op jit(solution)/shard_map/ppermute | solution.py:399
  168.7 1.2 copy-done.1
  169.9 0.8 copy-done.2
  170.7 8.2 %shard_map.240 = (bf16[256,512]{1,0:T(8,128)(2,1)}, bf16[256,512]{1,0:T(8,128)(2,1)}, bf16[256,512]{1,0:T(8,128)(2,1)}, bf16[256,512]{1,0:T(8,128)(2,1)}) custom-call(s32[5]{0:T(128)} %stack.27.c_ref.s_ref, bf16[272,512]{1,0:T(8,128)(2,1)} %get-tuple-element.43.rest_0_, bf16[272,512]{1,0:T(8,128)(2,1)} %copy-done.6, bf16[272,512]{1,0:T(8,128)(2,1)} %copy-done.8, ...), custom_call_target="tpu_custom_call" | custom-call | flops 3221225472 | bytes 21037076 | tf_op jit(solution)/shard_map/pallas_call | solution.py:55
  178.9 1.5 collective-permute-start.20
  180.4 2.1 collective-permute-start.22
  182.5 0.7 copy-done.4
  183.2 0.7 copy-done.5
  183.9 8.5 %shard_map.243 = (bf16[256,512]{1,0:T(8,128)(2,1)}, bf16[256,512]{1,0:T(8,128)(2,1)}, bf16[256,512]{1,0:T(8,128)(2,1)}, bf16[256,512]{1,0:T(8,128)(2,1)}) custom-call(s32[5]{0:T(128)} %stack.27.c_ref.s_ref, bf16[272,512]{1,0:T(8,128)(2,1)} %get-tuple-element.51.rest_0_, bf16[272,512]{1,0:T(8,128)(2,1)} %copy-done.7, bf16[272,512]{1,0:T(8,128)(2,1)} %copy-done.4, ...), custom_call_target="tpu_custom_call" | custom-call | flops 3221225472 | bytes 21037076 | tf_op jit(solution)/shard_map/pallas_call | solution.py:55
  192.4 1.5 collective-permute-start.31
  193.9 2.0 collective-permute-start.33
  196.8 4.1 %shard_map.241 = (bf16[256,512]{1,0:T(8,128)(2,1)}, bf16[256,512]{1,0:T(8,128)(2,1)}) custom-call(s32[5]{0:T(128)} %stack.27.c_ref.s_ref, bf16[256,512]{1,0:T(8,128)(2,1)} %get-tuple-element.45.rest_0_, bf16[256,512]{1,0:T(8,128)(2,1)} %copy-done.18, bf16[256,512]{1,0:T(8,128)(2,1)} %copy-done.19, bf16[256,512]{1,0:T(8,128)(2,1)} %copy-done.20, ...), custom_call_target="tpu_custom_call" | custom-call | flops 1000000000 | bytes 1589268 | tf_op jit(solution)/shard_map/pallas_call | solution.py:55
  200.9 3.5 %collective-permute-start.23 = (bf16[256,512]{1,0:T(8,128)(2,1)}, bf16[256,512]{1,0:T(8,128)(2,1)S(1)}, u32[]{:S(2)}, u32[]{:S(2)}) collective-permute-start(bf16[256,512]{1,0:T(8,128)(2,1)} %get-tuple-element.50), channel_id=1, source_target_pairs={{0,8},{4,12},{8,0},{12,4},{16,24},{20,28},{24,16},{28,20},{1,9},{5... | collective-permute-start | bytes 786440 | tf_op jit(solution)/shard_map/ppermute | solution.py:399
  205.3 4.1 %shard_map.244 = (bf16[256,512]{1,0:T(8,128)(2,1)}, bf16[256,512]{1,0:T(8,128)(2,1)}) custom-call(s32[5]{0:T(128)} %stack.27.c_ref.s_ref, bf16[256,512]{1,0:T(8,128)(2,1)} %get-tuple-element.53.rest_0_, bf16[256,512]{1,0:T(8,128)(2,1)} %copy-done.21, bf16[256,512]{1,0:T(8,128)(2,1)} %copy-done.22, bf16[256,512]{1,0:T(8,128)(2,1)} %copy-done.23, ...), custom_call_target="tpu_custom_call" | custom-call | flops 1000000000 | bytes 1589268 | tf_op jit(solution)/shard_map/pallas_call | solution.py:55
  209.4 4.9 %collective-permute-start.34 = (bf16[256,512]{1,0:T(8,128)(2,1)}, bf16[256,512]{1,0:T(8,128)(2,1)S(1)}, u32[]{:S(2)}, u32[]{:S(2)}) collective-permute-start(bf16[256,512]{1,0:T(8,128)(2,1)} %get-tuple-element.57), channel_id=1, source_target_pairs={{0,16},{4,20},{8,24},{12,28},{16,0},{20,4},{24,8},{28,12},{1,17},{... | collective-permute-start | bytes 786440 | tf_op jit(solution)/shard_map/ppermute | solution.py:399
  214.6 14.8 %collective-permute-done.34 = bf16[256,512]{1,0:T(8,128)(2,1)S(1)} collective-permute-done((bf16[256,512]{1,0:T(8,128)(2,1)}, bf16[256,512]{1,0:T(8,128)(2,1)S(1)}, u32[]{:S(2)}, u32[]{:S(2)}) %collective-permute-start.34) | collective-permute-done | bytes 262176 | tf_op jit(solution)/shard_map/ppermute | solution.py:399
  229.5 0.9 add_convert_fusion
  (110 shorter events, 6.9 us)
Async XLA Ops:
  2.8 12.4 %collective-permute-start = (bf16[8,1024]{1,0:T(8,128)(2,1)S(1)}, bf16[8,1024]{1,0:T(8,128)(2,1)S(1)}, u32[]{:S(2)}, u32[]{:S(2)}) collective-permute-start(bf16[8,1024]{1,0:T(8,128)(2,1)S(1)} %pad_maximum_fusion), channel_id=1, source_target_pairs={{0,4},{4,8},{8,12},{12,16},{16,20},{20,24},{24,28},{1,5},{5,9},{9,... | collective-permute-start | bytes 49160 | tf_op jit(solution)/shard_map/ppermute | solution.py:396
  5.2 31.7 %collective-permute-start.14 = (bf16[2048,512]{1,0:T(8,128)(2,1)}, bf16[2048,512]{1,0:T(8,128)(2,1)S(1)}, u32[]{:S(2)}, u32[]{:S(2)}) collective-permute-start(bf16[2048,512]{1,0:T(8,128)(2,1)} %bitcast.18), channel_id=1, source_target_pairs={{0,4},{1,5},{2,0},{3,1},{4,6},{5,7},{6,2},{7,3},{8,12},{9,13},{10,... | collective-permute-start | bytes 6291464 | tf_op jit(solution)/shard_map/ppermute | solution.py:433
  7.8 46.5 %collective-permute-start.15 = (bf16[2048,512]{1,0:T(8,128)(2,1)}, bf16[2048,512]{1,0:T(8,128)(2,1)}, u32[]{:S(2)}, u32[]{:S(2)}) collective-permute-start(bf16[2048,512]{1,0:T(8,128)(2,1)} %bitcast.21), channel_id=1, source_target_pairs={{0,4},{1,5},{2,0},{3,1},{4,6},{5,7},{6,2},{7,3},{8,12},{9,13},{10,... | collective-permute-start | bytes 6291464 | tf_op jit(solution)/shard_map/ppermute | solution.py:433
  9.1 67.7 %collective-permute-start.16 = (bf16[512,2048]{1,0:T(8,128)(2,1)}, bf16[512,2048]{1,0:T(8,128)(2,1)}, u32[]{:S(2)}, u32[]{:S(2)}) collective-permute-start(bf16[512,2048]{1,0:T(8,128)(2,1)} %bitcast.24), channel_id=1, source_target_pairs={{0,4},{1,5},{2,0},{3,1},{4,6},{5,7},{6,2},{7,3},{8,12},{9,13},{10,... | collective-permute-start | bytes 6291464 | tf_op jit(solution)/shard_map/ppermute | solution.py:433
  15.8 17.9 %copy-start.14 = (f32[2,4]{1,0:T(2,128)S(1)}, f32[2,4]{1,0:T(2,128)}, u32[]{:S(2)}) copy-start(f32[2,4]{1,0:T(2,128)} %param.35) | copy-start | bytes 100
  19.0 1.5 collective-permute-start.1
  21.7 6.9 %collective-permute-start.2 = (bf16[80,768]{1,0:T(8,128)(2,1)S(1)}, bf16[80,768]{1,0:T(8,128)(2,1)S(1)}, u32[]{:S(2)}, u32[]{:S(2)}) collective-permute-start(bf16[80,768]{1,0:T(8,128)(2,1)S(1)} %maximum_maximum_fusion), channel_id=1, source_target_pairs={{0,8},{4,12},{8,16},{12,20},{16,24},{20,28},{1,9},{5,13},{9,17},{1... | collective-permute-start | bytes 368648 | tf_op jit(solution)/shard_map/ppermute | solution.py:396
  25.2 9.2 %collective-permute-start.3 = (bf16[80,768]{1,0:T(8,128)(2,1)S(1)}, bf16[80,768]{1,0:T(8,128)(2,1)S(1)}, u32[]{:S(2)}, u32[]{:S(2)}) collective-permute-start(bf16[80,768]{1,0:T(8,128)(2,1)S(1)} %maximum_maximum_fusion), channel_id=1, source_target_pairs={{0,16},{4,20},{8,24},{12,28},{1,17},{5,21},{9,25},{13,29},{2,18},{... | collective-permute-start | bytes 368648 | tf_op jit(solution)/shard_map/ppermute | solution.py:396
  28.7 7.5 %collective-permute-start.4 = (bf16[80,768]{1,0:T(8,128)(2,1)S(1)}, bf16[80,768]{1,0:T(8,128)(2,1)S(1)}, u32[]{:S(2)}, u32[]{:S(2)}) collective-permute-start(bf16[80,768]{1,0:T(8,128)(2,1)S(1)} %maximum_maximum_fusion), channel_id=1, source_target_pairs={{0,24},{4,28},{1,25},{5,29},{2,26},{6,30},{3,27},{7,31}} | collective-permute-start | bytes 368648 | tf_op jit(solution)/shard_map/ppermute | solution.py:396
  36.9 47.0 %collective-permute-start.5 = (bf16[64,768]{1,0:T(8,128)(2,1)S(1)}, bf16[64,768]{1,0:T(8,128)(2,1)S(1)}, u32[]{:S(2)}, u32[]{:S(2)}) collective-permute-start(bf16[64,768]{1,0:T(8,128)(2,1)S(1)} %get-tuple-element.65), channel_id=1, source_target_pairs={{0,4},{4,0},{8,12},{12,8},{16,20},{20,16},{24,28},{28,24},{1,5},{5... | collective-permute-start | bytes 294920 | tf_op jit(solution)/shard_map/ppermute | solution.py:399
  36.9 47.0 %copy-start = (bf16[2048,512]{1,0:T(8,128)(2,1)}, bf16[2048,512]{1,0:T(8,128)(2,1)S(1)}, u32[]{:S(2)}) copy-start(bf16[2048,512]{1,0:T(8,128)(2,1)S(1)} %collective-permute-done.14.rest_7_) | copy-start | bytes 6291460
  36.9 131.7 %collective-permute-start.17 = (bf16[2048,512]{1,0:T(8,128)(2,1)S(1)}, bf16[2048,512]{1,0:T(8,128)(2,1)S(1)}, u32[]{:S(2)}, u32[]{:S(2)}) collective-permute-start(bf16[2048,512]{1,0:T(8,128)(2,1)S(1)} %collective-permute-done.14.rest_7_), channel_id=1, source_target_pairs={{0,4},{1,5},{6,2},{7,3},{8,12},{9,13},{14,10},{15,11},{16,20},{17,... | collective-permute-start | bytes 6291464 | tf_op jit(solution)/shard_map/ppermute | solution.py:434
  54.3 114.3 %collective-permute-start.18 = (bf16[2048,512]{1,0:T(8,128)(2,1)}, bf16[2048,512]{1,0:T(8,128)(2,1)S(1)}, u32[]{:S(2)}, u32[]{:S(2)}) collective-permute-start(bf16[2048,512]{1,0:T(8,128)(2,1)} %collective-permute-done.15.rest_8_), channel_id=1, source_target_pairs={{0,4},{1,5},{6,2},{7,3},{8,12},{9,13},{14,10},{15,11},{16,20},{17,... | collective-permute-start | bytes 6291464 | tf_op jit(solution)/shard_map/ppermute | solution.py:434
  76.8 91.9 %collective-permute-start.19 = (bf16[512,2048]{1,0:T(8,128)(2,1)}, bf16[512,2048]{1,0:T(8,128)(2,1)}, u32[]{:S(2)}, u32[]{:S(2)}) collective-permute-start(bf16[512,2048]{1,0:T(8,128)(2,1)} %collective-permute-done.16.rest_9_), channel_id=1, source_target_pairs={{0,4},{1,5},{6,2},{7,3},{8,12},{9,13},{14,10},{15,11},{16,20},{17,... | collective-permute-start | bytes 6291464 | tf_op jit(solution)/shard_map/ppermute | solution.py:434
  84.5 14.3 %copy-start.12 = (s32[256,3]{0,1:T(4,128)S(1)}, s32[256,3]{0,1:T(4,128)}, u32[]{:S(2)}) copy-start(s32[256,3]{0,1:T(4,128)} %param.45) | copy-start | bytes 9220
  92.2 20.4 %copy-start.13 = (f32[256,3]{0,1:T(4,128)S(1)}, f32[256,3]{0,1:T(4,128)}, u32[]{:S(2)}) copy-start(f32[256,3]{0,1:T(4,128)} %param.46) | copy-start | bytes 9220
  92.2 6.6 %collective-permute-start.6 = (bf16[256,512]{1,0:T(8,128)(2,1)}, bf16[256,512]{1,0:T(8,128)(2,1)S(1)}, u32[]{:S(2)}, u32[]{:S(2)}) collective-permute-start(bf16[256,512]{1,0:T(8,128)(2,1)} %get-tuple-element.38), channel_id=1, source_target_pairs={{0,1},{1,0},{2,3},{3,2},{4,5},{5,4},{6,7},{7,6},{8,9},{9,8},{10,11... | collective-permute-start | bytes 786440 | tf_op jit(solution)/shard_map/ppermute | solution.py:399
  93.7 13.6 %collective-permute-start.7 = (bf16[256,512]{1,0:T(8,128)(2,1)}, bf16[256,512]{1,0:T(8,128)(2,1)S(1)}, u32[]{:S(2)}, u32[]{:S(2)}) collective-permute-start(bf16[256,512]{1,0:T(8,128)(2,1)} %get-tuple-element.39), channel_id=1, source_target_pairs={{0,2},{1,3},{2,0},{3,1},{4,6},{5,7},{6,4},{7,5},{8,10},{9,11},{10,... | collective-permute-start | bytes 786440 | tf_op jit(solution)/shard_map/ppermute | solution.py:399
  98.8 8.5 %copy-start.24 = (bf16[256,512]{1,0:T(8,128)(2,1)}, bf16[256,512]{1,0:T(8,128)(2,1)S(1)}, u32[]{:S(2)}) copy-start(bf16[256,512]{1,0:T(8,128)(2,1)S(1)} %collective-permute-done.6.rest_1_) | copy-start | bytes 786436
  98.8 8.5 %collective-permute-start.8 = (bf16[256,512]{1,0:T(8,128)(2,1)}, bf16[256,512]{1,0:T(8,128)(2,1)S(1)}, u32[]{:S(2)}, u32[]{:S(2)}) collective-permute-start(bf16[256,512]{1,0:T(8,128)(2,1)} %get-tuple-element.40), channel_id=1, source_target_pairs={{0,3},{1,2},{2,1},{3,0},{4,7},{5,6},{6,5},{7,4},{8,11},{9,10},{10,... | collective-permute-start | bytes 786440 | tf_op jit(solution)/shard_map/ppermute | solution.py:399
  107.3 0.8 copy-start.26
  111.0 19.1 %collective-permute-start.9 = (bf16[272,512]{1,0:T(8,128)(2,1)}, bf16[272,512]{1,0:T(8,128)(2,1)S(1)}, u32[]{:S(2)}, u32[]{:S(2)}) collective-permute-start(bf16[272,512]{1,0:T(8,128)(2,1)} %get-tuple-element.42.rest_0_), channel_id=1, source_target_pairs={{0,8},{4,12},{8,0},{12,4},{16,24},{20,28},{24,16},{28,20},{1,9},{5... | collective-permute-start | bytes 835592 | tf_op jit(solution)/shard_map/ppermute | solution.py:399
  112.6 20.0 %copy-start.11 = (f32[8,256]{1,0:T(8,128)}, f32[8,256]{1,0:T(8,128)S(1)}, u32[]{:S(2)}) copy-start(f32[8,256]{1,0:T(8,128)S(1)} %select_maximum_fusion.rest_2_.rest_4_) | copy-start | bytes 24580
  112.6 5.9 %collective-permute-start.10 = (f32[8,256]{1,0:T(8,128)S(1)}, f32[8,256]{1,0:T(8,128)S(1)}, u32[]{:S(2)}, u32[]{:S(2)}) collective-permute-start(f32[8,256]{1,0:T(8,128)S(1)} %select_maximum_fusion.rest_2_.rest_4_), channel_id=1, source_target_pairs={{0,8},{4,12},{8,0},{12,4},{16,24},{20,28},{24,16},{28,20},{1,9},{5... | collective-permute-start | bytes 24584 | tf_op jit(solution)/shard_map/ppermute | solution.py:399
  118.5 14.1 %copy-start.31 = (f32[8,256]{1,0:T(8,128)}, f32[8,256]{1,0:T(8,128)S(1)}, u32[]{:S(2)}) copy-start(f32[8,256]{1,0:T(8,128)S(1)} %collective-permute-done.10.rest_3_.rest_5_) | copy-start | bytes 24580
  118.5 4.5 %collective-permute-start.26 = (f32[8,256]{1,0:T(8,128)S(1)}, f32[8,256]{1,0:T(8,128)S(1)}, u32[]{:S(2)}, u32[]{:S(2)}) collective-permute-start(f32[8,256]{1,0:T(8,128)S(1)} %select_maximum_fusion.rest_2_.rest_4_), channel_id=1, source_target_pairs={{0,16},{4,20},{8,24},{12,28},{16,0},{20,4},{24,8},{28,12},{1,17},{... | collective-permute-start | bytes 24584 | tf_op jit(solution)/shard_map/ppermute | solution.py:399
  123.1 36.5 %copy-start.29 = (f32[8,256]{1,0:T(8,128)}, f32[8,256]{1,0:T(8,128)S(1)}, u32[]{:S(2)}) copy-start(f32[8,256]{1,0:T(8,128)S(1)} %collective-permute-done.26.rest_2_.rest_4_) | copy-start | bytes 24580
  123.1 5.5 %collective-permute-start.27 = (f32[8,256]{1,0:T(8,128)S(1)}, f32[8,256]{1,0:T(8,128)S(1)}, u32[]{:S(2)}, u32[]{:S(2)}) collective-permute-start(f32[8,256]{1,0:T(8,128)S(1)} %select_maximum_fusion.rest_2_.rest_4_), channel_id=1, source_target_pairs={{0,24},{4,28},{8,16},{12,20},{16,8},{20,12},{24,0},{28,4},{1,25},{... | collective-permute-start | bytes 24584 | tf_op jit(solution)/shard_map/ppermute | solution.py:399
  128.6 31.0 %copy-start.30 = (f32[8,256]{1,0:T(8,128)}, f32[8,256]{1,0:T(8,128)S(1)}, u32[]{:S(2)}) copy-start(f32[8,256]{1,0:T(8,128)S(1)} %collective-permute-done.27.rest_3_.rest_5_) | copy-start | bytes 24580
  128.6 18.6 %collective-permute-start.24 = (bf16[272,512]{1,0:T(8,128)(2,1)}, bf16[272,512]{1,0:T(8,128)(2,1)S(1)}, u32[]{:S(2)}, u32[]{:S(2)}) collective-permute-start(bf16[272,512]{1,0:T(8,128)(2,1)} %get-tuple-element.42.rest_0_), channel_id=1, source_target_pairs={{0,16},{4,20},{8,24},{12,28},{16,0},{20,4},{24,8},{28,12},{1,17},{... | collective-permute-start | bytes 835592 | tf_op jit(solution)/shard_map/ppermute | solution.py:399
  130.2 2.4 %copy-start.15 = (bf16[272,512]{1,0:T(8,128)(2,1)}, bf16[272,512]{1,0:T(8,128)(2,1)S(1)}, u32[]{:S(2)}) copy-start(bf16[272,512]{1,0:T(8,128)(2,1)S(1)} %collective-permute-done.9.rest_1_) | copy-start | bytes 835588
  130.2 18.2 %collective-permute-start.25 = (bf16[272,512]{1,0:T(8,128)(2,1)}, bf16[272,512]{1,0:T(8,128)(2,1)S(1)}, u32[]{:S(2)}, u32[]{:S(2)}) collective-permute-start(bf16[272,512]{1,0:T(8,128)(2,1)} %get-tuple-element.42.rest_0_), channel_id=1, source_target_pairs={{0,24},{4,28},{8,16},{12,20},{16,8},{20,12},{24,0},{28,4},{1,25},{... | collective-permute-start | bytes 835592 | tf_op jit(solution)/shard_map/ppermute | solution.py:399
  147.2 12.4 %copy-start.16 = (bf16[272,512]{1,0:T(8,128)(2,1)}, bf16[272,512]{1,0:T(8,128)(2,1)S(1)}, u32[]{:S(2)}) copy-start(bf16[272,512]{1,0:T(8,128)(2,1)S(1)} %collective-permute-done.24.rest_0_) | copy-start | bytes 835588
  147.2 7.1 %collective-permute-start.11 = (bf16[272,512]{1,0:T(8,128)(2,1)}, bf16[272,512]{1,0:T(8,128)(2,1)S(1)}, u32[]{:S(2)}, u32[]{:S(2)}) collective-permute-start(bf16[272,512]{1,0:T(8,128)(2,1)} %get-tuple-element.43.rest_0_), channel_id=1, source_target_pairs={{0,1},{1,0},{2,3},{3,2},{4,5},{5,4},{6,7},{7,6},{8,9},{9,8},{10,11... | collective-permute-start | bytes 835592 | tf_op jit(solution)/shard_map/ppermute | solution.py:399
  148.3 11.3 %copy-start.17 = (bf16[272,512]{1,0:T(8,128)(2,1)}, bf16[272,512]{1,0:T(8,128)(2,1)S(1)}, u32[]{:S(2)}) copy-start(bf16[272,512]{1,0:T(8,128)(2,1)S(1)} %collective-permute-done.25.rest_1_) | copy-start | bytes 835588
  148.3 14.2 %collective-permute-start.12 = (bf16[272,512]{1,0:T(8,128)(2,1)}, bf16[272,512]{1,0:T(8,128)(2,1)S(1)}, u32[]{:S(2)}, u32[]{:S(2)}) collective-permute-start(bf16[272,512]{1,0:T(8,128)(2,1)} %get-tuple-element.44), channel_id=1, source_target_pairs={{0,2},{1,3},{2,0},{3,1},{4,6},{5,7},{6,4},{7,5},{8,10},{9,11},{10,... | collective-permute-start | bytes 835592 | tf_op jit(solution)/shard_map/ppermute | solution.py:399
  154.3 14.4 %copy-start.6 = (bf16[272,512]{1,0:T(8,128)(2,1)}, bf16[272,512]{1,0:T(8,128)(2,1)S(1)}, u32[]{:S(2)}) copy-start(bf16[272,512]{1,0:T(8,128)(2,1)S(1)} %collective-permute-done.11.rest_1_) | copy-start | bytes 835588
  154.3 11.0 %collective-permute-start.13 = (bf16[272,512]{1,0:T(8,128)(2,1)}, bf16[272,512]{1,0:T(8,128)(2,1)S(1)}, u32[]{:S(2)}, u32[]{:S(2)}) collective-permute-start(bf16[272,512]{1,0:T(8,128)(2,1)} %get-tuple-element.44), channel_id=1, source_target_pairs={{0,3},{1,2},{2,1},{3,0},{4,7},{5,6},{6,5},{7,4},{8,11},{9,10},{10,... | collective-permute-start | bytes 835592 | tf_op jit(solution)/shard_map/ppermute | solution.py:399
  162.5 6.2 %copy-start.8 = (bf16[272,512]{1,0:T(8,128)(2,1)}, bf16[272,512]{1,0:T(8,128)(2,1)S(1)}, u32[]{:S(2)}) copy-start(bf16[272,512]{1,0:T(8,128)(2,1)S(1)} %collective-permute-done.12.rest_2_) | copy-start | bytes 835588
  162.5 20.0 %collective-permute-start.29 = (bf16[272,512]{1,0:T(8,128)(2,1)}, bf16[272,512]{1,0:T(8,128)(2,1)S(1)}, u32[]{:S(2)}, u32[]{:S(2)}) collective-permute-start(bf16[272,512]{1,0:T(8,128)(2,1)} %get-tuple-element.52), channel_id=1, source_target_pairs={{0,2},{1,3},{2,0},{3,1},{4,6},{5,7},{6,4},{7,5},{8,10},{9,11},{10,... | collective-permute-start | bytes 835592 | tf_op jit(solution)/shard_map/ppermute | solution.py:399
  165.3 3.4 %copy-start.9 = (bf16[272,512]{1,0:T(8,128)(2,1)}, bf16[272,512]{1,0:T(8,128)(2,1)S(1)}, u32[]{:S(2)}) copy-start(bf16[272,512]{1,0:T(8,128)(2,1)S(1)} %collective-permute-done.13.rest_3_) | copy-start | bytes 835588
  165.3 17.2 %collective-permute-start.30 = (bf16[272,512]{1,0:T(8,128)(2,1)}, bf16[272,512]{1,0:T(8,128)(2,1)S(1)}, u32[]{:S(2)}, u32[]{:S(2)}) collective-permute-start(bf16[272,512]{1,0:T(8,128)(2,1)} %get-tuple-element.52), channel_id=1, source_target_pairs={{0,3},{1,2},{2,1},{3,0},{4,7},{5,6},{6,5},{7,4},{8,11},{9,10},{10,... | collective-permute-start | bytes 835592 | tf_op jit(solution)/shard_map/ppermute | solution.py:399
  168.6 1.3 copy-start.1
  168.6 11.8 %collective-permute-start.28 = (bf16[272,512]{1,0:T(8,128)(2,1)}, bf16[272,512]{1,0:T(8,128)(2,1)S(1)}, u32[]{:S(2)}, u32[]{:S(2)}) collective-permute-start(bf16[272,512]{1,0:T(8,128)(2,1)} %get-tuple-element.51.rest_0_), channel_id=1, source_target_pairs={{0,1},{1,0},{2,3},{3,2},{4,5},{5,4},{6,7},{7,6},{8,9},{9,8},{10,11... | collective-permute-start | bytes 835592 | tf_op jit(solution)/shard_map/ppermute | solution.py:399
  168.6 2.1 copy-start.2
  178.9 15.0 %collective-permute-start.20 = (bf16[256,512]{1,0:T(8,128)(2,1)}, bf16[256,512]{1,0:T(8,128)(2,1)S(1)}, u32[]{:S(2)}, u32[]{:S(2)}) collective-permute-start(bf16[256,512]{1,0:T(8,128)(2,1)} %get-tuple-element.46), channel_id=1, source_target_pairs={{0,1},{1,0},{2,3},{3,2},{4,5},{5,4},{6,7},{7,6},{8,9},{9,8},{10,11... | collective-permute-start | bytes 786440 | tf_op jit(solution)/shard_map/ppermute | solution.py:399
  180.4 15.6 %collective-permute-start.21 = (bf16[256,512]{1,0:T(8,128)(2,1)}, bf16[256,512]{1,0:T(8,128)(2,1)S(1)}, u32[]{:S(2)}, u32[]{:S(2)}) collective-permute-start(bf16[256,512]{1,0:T(8,128)(2,1)} %get-tuple-element.47), channel_id=1, source_target_pairs={{0,2},{1,3},{2,0},{3,1},{4,6},{5,7},{6,4},{7,5},{8,10},{9,11},{10,... | collective-permute-start | bytes 786440 | tf_op jit(solution)/shard_map/ppermute | solution.py:399
  180.4 2.1 copy-start.7
  180.4 15.6 %collective-permute-start.22 = (bf16[256,512]{1,0:T(8,128)(2,1)}, bf16[256,512]{1,0:T(8,128)(2,1)S(1)}, u32[]{:S(2)}, u32[]{:S(2)}) collective-permute-start(bf16[256,512]{1,0:T(8,128)(2,1)} %get-tuple-element.48), channel_id=1, source_target_pairs={{0,3},{1,2},{2,1},{3,0},{4,7},{5,6},{6,5},{7,4},{8,11},{9,10},{10,... | collective-permute-start | bytes 786440 | tf_op jit(solution)/shard_map/ppermute | solution.py:399
  182.5 0.7 copy-start.4
  183.2 0.7 copy-start.5
  192.4 12.0 %collective-permute-start.31 = (bf16[256,512]{1,0:T(8,128)(2,1)}, bf16[256,512]{1,0:T(8,128)(2,1)S(1)}, u32[]{:S(2)}, u32[]{:S(2)}) collective-permute-start(bf16[256,512]{1,0:T(8,128)(2,1)} %get-tuple-element.54), channel_id=1, source_target_pairs={{0,1},{1,0},{2,3},{3,2},{4,5},{5,4},{6,7},{7,6},{8,9},{9,8},{10,11... | collective-permute-start | bytes 786440 | tf_op jit(solution)/shard_map/ppermute | solution.py:399
  193.9 10.6 %collective-permute-start.32 = (bf16[256,512]{1,0:T(8,128)(2,1)}, bf16[256,512]{1,0:T(8,128)(2,1)S(1)}, u32[]{:S(2)}, u32[]{:S(2)}) collective-permute-start(bf16[256,512]{1,0:T(8,128)(2,1)} %get-tuple-element.55), channel_id=1, source_target_pairs={{0,2},{1,3},{2,0},{3,1},{4,6},{5,7},{6,4},{7,5},{8,10},{9,11},{10,... | collective-permute-start | bytes 786440 | tf_op jit(solution)/shard_map/ppermute | solution.py:399
  193.9 2.1 copy-start.18
  193.9 10.5 %collective-permute-start.33 = (bf16[256,512]{1,0:T(8,128)(2,1)}, bf16[256,512]{1,0:T(8,128)(2,1)S(1)}, u32[]{:S(2)}, u32[]{:S(2)}) collective-permute-start(bf16[256,512]{1,0:T(8,128)(2,1)} %get-tuple-element.56), channel_id=1, source_target_pairs={{0,3},{1,2},{2,1},{3,0},{4,7},{5,6},{6,5},{7,4},{8,11},{9,10},{10,... | collective-permute-start | bytes 786440 | tf_op jit(solution)/shard_map/ppermute | solution.py:399
  196.0 0.8 copy-start.20
  200.9 28.6 %copy-start.3 = (f32[256,512]{1,0:T(8,128)S(1)}, f32[256,512]{1,0:T(8,128)}, u32[]{:S(2)}) copy-start(f32[256,512]{1,0:T(8,128)} %get-tuple-element.41) | copy-start | bytes 1572868
  200.9 28.6 %copy-start.10 = (bf16[256,512]{1,0:T(8,128)(2,1)S(1)}, bf16[256,512]{1,0:T(8,128)(2,1)}, u32[]{:S(2)}) copy-start(bf16[256,512]{1,0:T(8,128)(2,1)} %get-tuple-element.49) | copy-start | bytes 786436
  200.9 13.8 %collective-permute-start.23 = (bf16[256,512]{1,0:T(8,128)(2,1)}, bf16[256,512]{1,0:T(8,128)(2,1)S(1)}, u32[]{:S(2)}, u32[]{:S(2)}) collective-permute-start(bf16[256,512]{1,0:T(8,128)(2,1)} %get-tuple-element.50), channel_id=1, source_target_pairs={{0,8},{4,12},{8,0},{12,4},{16,24},{20,28},{24,16},{28,20},{1,9},{5... | collective-permute-start | bytes 786440 | tf_op jit(solution)/shard_map/ppermute | solution.py:399
  204.4 0.7 copy-start.21
  204.4 0.8 copy-start.22
  204.5 0.9 copy-start.23
  209.4 20.0 %collective-permute-start.34 = (bf16[256,512]{1,0:T(8,128)(2,1)}, bf16[256,512]{1,0:T(8,128)(2,1)S(1)}, u32[]{:S(2)}, u32[]{:S(2)}) collective-permute-start(bf16[256,512]{1,0:T(8,128)(2,1)} %get-tuple-element.57), channel_id=1, source_target_pairs={{0,16},{4,20},{8,24},{12,28},{16,0},{20,4},{24,8},{28,12},{1,17},{... | collective-permute-start | bytes 786440 | tf_op jit(solution)/shard_map/ppermute | solution.py:399
  214.3 15.1 %collective-permute-start.35 = (bf16[256,512]{1,0:T(8,128)(2,1)}, bf16[256,512]{1,0:T(8,128)(2,1)S(1)}, u32[]{:S(2)}, u32[]{:S(2)}) collective-permute-start(bf16[256,512]{1,0:T(8,128)(2,1)} %get-tuple-element.58), channel_id=1, source_target_pairs={{0,24},{4,28},{8,16},{12,20},{16,8},{20,12},{24,0},{28,4},{1,25},{... | collective-permute-start | bytes 786440 | tf_op jit(solution)/shard_map/ppermute | solution.py:399
  (4 other events, 2.6 us)
